TPU v7x, 32 devices: a whole 2x2x4 slice. The times are simulated.
32 devices in a mesh: sp: 8 (over z, y), tp: 4 (over x, core).
Axes of the slice: x: 2, y: 2, z: 4, core: 2. Of those that a mesh axis runs over, the one named last changes fastest.
Arguments:
- layer_input_rows: bfloat16 [2048, 2048], P('sp'), may hold values from -6 to 6
- input_norm_gain: float32 [2048], replicated, may hold values from 0.1 to 1.9
- query_weight: bfloat16 [2048, 1024], P(None, 'tp'), may hold values from -0.125 to 0.125
- key_weight: bfloat16 [2048, 1024], P(None, 'tp'), may hold values from -0.125 to 0.125
- value_weight: bfloat16 [2048, 1024], P(None, 'tp'), may hold values from -0.125 to 0.125
- query_norm_gain: float32 [64], replicated, may hold values from 0.5 to 9
- key_norm_gain: float32 [64], replicated, may hold values from 0.5 to 9
- cumulative_gate: float32 [2048, 16], P('sp', 'tp'), may hold values from -288.72 to 0, as said below
- attention_norm_gain: float32 [1024], P('tp'), may hold values from 0.1 to 1.9
- recurrence_query_weight: bfloat16 [2048, 1024], P(None, 'tp'), may hold values from -0.125 to 0.125
- forget_weight: bfloat16 [2048, 1024], P(None, 'tp'), may hold values from -0.125 to 0.125
- recurrence_value_weight: bfloat16 [2048, 1024], P(None, 'tp'), may hold values from -0.125 to 0.125
- output_gate_weight: bfloat16 [2048, 1024], P(None, 'tp'), may hold values from -0.125 to 0.125
- gate_lower_slack: float32 [1024], P('tp'), may hold values from 0 to 0.06
- extra_log_decay: float32 [2048, 8], P('sp', 'tp'), may hold values from -1.5 to 0
- recurrence_norm_gain: float32 [1024], P('tp'), may hold values from 0.1 to 1.9
- attention_output_weight: bfloat16 [1024, 2048], P('tp'), may hold values from -0.125 to 0.125
- recurrence_output_weight: bfloat16 [1024, 2048], P('tp'), may hold values from -0.125 to 0.125
Outputs:
- mixed: bfloat16 [2048, 2048], P(('sp', 'tp'))
- log_sum: float32 [2048, 16], P('sp', 'tp')
Inputs may be any that keep to these rules, and one draw needn't show every extreme that they name: `cumulative_gate`: each column never rises along positions.
All inputs are finite; a program needn't handle non-finite values.
Results may differ from a plain program's by a relative error of at most 0.015.
The roundings to bfloat16 on the way count: a program that leaves them out, or rounds other values in their place, can miss the bound.
Values may be sent and summed in bfloat16 or wider, within the bound.
A program may use at most 64 MiB of HBM per device.

v0:
```python
import functools
import math

import jax
import jax.numpy as jnp
from jax import lax
from jax.experimental import pallas as pl
from jax.experimental.pallas import tpu as pltpu
from jax.sharding import PartitionSpec as P

HEAD_DIM = 64
STATE_ROWS = 128
LANES = 128
EPSILON = 1e-06
HIGHEST = lax.Precision.HIGHEST
MESH = pl.DeviceIdType.MESH
F32 = jnp.float32
BF16 = jnp.bfloat16


def dot(a, b):
    return jnp.dot(a, b, preferred_element_type=F32)


def dot_exact(a, b):
    return jnp.dot(a, b, preferred_element_type=F32, precision=HIGHEST)


def dot_nt(a, b, precision=None):
    return lax.dot_general(
        a, b, (((1,), (1,)), ((), ())), preferred_element_type=F32, precision=precision
    )


def iota(shape, axis):
    return lax.broadcasted_iota(jnp.int32, shape, axis)


def grid_of(count):
    columns = max(c for c in range(1, math.isqrt(count) + 1) if count % c == 0)
    return count // columns, columns


def kernel(
    sizes,
    x_hbm, wk_hbm, wv_hbm, wf_hbm, wrv_hbm, wrq_hbm, wq_hbm, wog_hbm, wao_hbm, wro_hbm,
    in_gain_hbm, q_gain_hbm, k_gain_hbm, gate_t_hbm, a_gain_hbm,
    slack_hbm, extra_t_hbm, r_gain_hbm,
    mixed_ref, logsum_ref,
    x_v, wk_v, wv_v, wf_v, wrv_v, wrq_v, wq_v, wog_v, wao_v, wro_v,
    xn, kv, gates, q_t, m_s, l_s, acc, attn_t,
    inner, vq, og, ext, st, chain_in, chain_out, incoming, part, send2, recv1, recv2,
    in_gain, q_gain, k_gain, gate_t, a_gain, slack, extra_t, r_gain, rec_part,
    load_sem, col_send, row_send, recv_sem, st_send, st_recv, chain_send, chain_recv,
    s1_send, s1_recv, s2_send, s2_recv,
):
    nz, ny, ntp = sizes
    rows, width = x_v.shape
    cols = wk_v.shape[1]
    heads = cols // HEAD_DIM
    pairs = cols // LANES
    rec_heads = cols // STATE_ROWS
    chips = ntp // 2
    rb = rows // ntp
    pieces = rows // LANES
    splits = s1_send.shape[1]
    part_cols = width // splits

    sp, tp = lax.axis_index("sp"), lax.axis_index("tp")
    z, y = sp // ny, sp % ny
    chip, core = tp // 2, tp % 2
    partner = chip * 2 + (1 - core)

    loads = []
    for i, (src, dst) in enumerate((
        (x_hbm, x_v), (wk_hbm, wk_v), (wv_hbm, wv_v), (wf_hbm, wf_v), (wrv_hbm, wrv_v),
        (wrq_hbm, wrq_v), (wq_hbm, wq_v), (wog_hbm, wog_v), (wao_hbm, wao_v), (wro_hbm, wro_v),
        (in_gain_hbm, in_gain), (q_gain_hbm, q_gain), (k_gain_hbm, k_gain),
        (gate_t_hbm, gate_t), (a_gain_hbm, a_gain), (slack_hbm, slack),
        (extra_t_hbm, extra_t), (r_gain_hbm, r_gain),
    )):
        loads.append(pltpu.make_async_copy(src, dst, load_sem.at[i]))

    for copy in loads[:3] + loads[10:]:
        copy.start()

    barrier = pltpu.get_barrier_semaphore()

    def greet(where):
        pl.semaphore_signal(barrier, inc=1, device_id=where, device_id_type=MESH)

    @pl.when(z > 0)
    def _():
        greet((sp - ny, tp))

    @pl.when(z < nz - 1)
    def _():
        greet((sp + ny, tp))

    for k in range(1, ny):
        greet((z * ny + (y + k) % ny, tp))
    greet((sp, partner))
    for k in range(1, chips):
        greet((sp, ((chip + k) % chips) * 2 + core))

    loads[0].wait()
    for copy in loads[10:]:
        copy.wait()
    for copy in loads[3:6]:
        copy.start()
    xf = x_v[...].astype(F32)
    scale = lax.rsqrt(jnp.mean(xf * xf, axis=-1, keepdims=True) + EPSILON)
    xn[...] = (xf * scale * in_gain[...]).astype(BF16)

    block_ones = jnp.where(
        iota((cols, cols), 0) // HEAD_DIM == iota((cols, cols), 1) // HEAD_DIM, 1.0 / HEAD_DIM, 0.0
    ).astype(F32)
    repeat = (iota((HEAD_DIM, cols), 1) % HEAD_DIM == iota((HEAD_DIM, cols), 0)).astype(F32)

    def head_norm(v, gain_ref):
        mean = dot_exact(v * v, block_ones)
        gain = dot_exact(jnp.broadcast_to(gain_ref[...], (8, HEAD_DIM)), repeat)[0:1]
        return v * lax.rsqrt(mean + EPSILON) * gain

    loads[1].wait()
    keys = head_norm(dot(xn[...], wk_v[...]), k_gain).astype(BF16)
    for p in range(pairs):
        kv[sp, 2 * p] = keys[:, p * LANES : (p + 1) * LANES]
    gates[sp] = jnp.zeros((8, rows), F32)
    gates[sp, 0:heads, :] = gate_t[...]

    def piece(slot, i):
        return gates.at[slot] if i == 0 else kv.at[slot, i - 1]

    def piece_copy(slot, i, send, where):
        return pltpu.make_async_remote_copy(
            src_ref=piece(slot, i), dst_ref=piece(slot, i), send_sem=send.at[i],
            recv_sem=recv_sem.at[slot, i], device_id=where, device_id_type=MESH,
        )

    every = range(1 + 2 * pairs)

    def pieces_of(p):
        return ((0,) if p == 0 else ()) + (1 + 2 * p, 2 + 2 * p)

    def up_copy(source_z, i):
        return piece_copy(source_z * ny + y, i, col_send.at[source_z], (sp + ny, tp))

    def side_copy(source_z, k, i):
        where = (z * ny + (y + k) % ny, tp)
        return piece_copy(source_z * ny + y, i, row_send.at[source_z, k], where)

    def wait_pieces(slot, which):
        for i in which:
            piece_copy(slot, i, col_send.at[0], (sp, partner)).wait_recv()

    def pass_on(source_z, p):
        for i in pieces_of(p):
            wait_pieces(source_z * ny + y, (i,))

            @pl.when(z < nz - 1)
            def _():
                up_copy(source_z, i).start()

            for k in range(1, ny):
                side_copy(source_z, k, i).start()

    greeted = (ny - 1) + chips + (z > 0).astype(jnp.int32) + (z < nz - 1).astype(jnp.int32)
    pl.semaphore_wait(barrier, greeted)

    def start_own(which):
        @pl.when(z < nz - 1)
        def _():
            for i in which:
                up_copy(z, i).start()

        for k in range(1, ny):
            @pl.when(y + k < ny)
            def _():
                for i in which:
                    side_copy(z, k, i).start()

    start_own([0] + [1 + 2 * p for p in range(pairs)])

    loads[2].wait()
    for copy in loads[6:10]:
        copy.start()
    values_t = dot(xn[...], wv_v[...]).T.astype(BF16)
    for p in range(pairs):
        for i in range(pieces):
            kv[sp, 2 * p + 1, i * LANES : (i + 1) * LANES, :] = values_t[
                p * LANES : (p + 1) * LANES, i * LANES : (i + 1) * LANES
            ]
    start_own([2 + 2 * p for p in range(pairs)])

    tri = (iota((rows, rows), 0) >= iota((rows, rows), 1)).astype(F32)
    loads[3].wait()
    share = slack[...] / (1.0 + jnp.exp(dot(xn[...], wf_v[...])))
    run = dot_exact(tri, jnp.log1p(-share))
    ext[...] = jnp.zeros_like(ext)
    ext[0:rec_heads, :] = extra_t[...]
    ext_row = dot_nt(ext[...], tri, HIGHEST)
    ext_col = dot_nt(tri, ext[...], HIGHEST)
    loads[4].wait()
    rec_value = dot(xn[...], wrv_v[...])
    loads[5].wait()
    rec_query = dot(xn[...], wrq_v[...])
    rec_query = rec_query / (1.0 + jnp.exp(-rec_query))
    grown = rec_query * jnp.exp(run)
    last = run[rows - 1 : rows]
    st_rows = STATE_ROWS + 16
    for j in range(rec_heads):
        lanes = slice(j * STATE_ROWS, (j + 1) * STATE_ROWS)
        e_col = ext_col[:, j : j + 1]
        e_row = ext_row[j : j + 1, :]
        e_last = e_row[:, rows - 1 : rows]
        value = rec_value[:, lanes].astype(BF16)
        left = share[:, lanes] * jnp.exp(last[:, lanes] - run[:, lanes] + (e_last - e_col))
        st[y, j * st_rows : j * st_rows + STATE_ROWS, :] = dot(
            rec_value[:, lanes].T.astype(BF16), left.astype(BF16)
        ).astype(BF16)
        st[y, j * st_rows + STATE_ROWS : (j + 1) * st_rows, :] = jnp.broadcast_to(
            jnp.exp(last[:, lanes] + e_last), (16, STATE_ROWS)
        ).astype(BF16)
        scores = dot_nt(
            grown[:, lanes].astype(BF16), (share[:, lanes] * jnp.exp(-run[:, lanes])).astype(BF16)
        )
        fading = jnp.exp(jnp.where(tri > 0.5, e_col - e_row, -jnp.inf))
        scores = jnp.where(tri > 0.5, scores * fading, 0.0)
        inner[:, lanes] = dot(scores.astype(BF16), value)
        vq[:, lanes] = (grown[:, lanes] * jnp.exp(e_col)).astype(BF16)

    def st_copy(k):
        return pltpu.make_async_remote_copy(
            src_ref=st.at[y], dst_ref=st.at[y], send_sem=st_send.at[k], recv_sem=st_recv.at[y],
            device_id=(z * ny + (y + k) % ny, tp), device_id_type=MESH,
        )

    for k in range(1, ny):
        st_copy(k).start()

    @pl.when(z > 0)
    def _():
        for p in range(pairs):
            pass_on(z - 1, p)

    loads[6].wait()
    queries_t = (head_norm(dot(xn[...], wq_v[...]), q_gain).astype(BF16).astype(F32)).T
    half_of = iota((LANES, rows), 0) // HEAD_DIM
    for h in range(heads):
        pair = queries_t[(h // 2) * LANES : (h // 2 + 1) * LANES, :] * HEAD_DIM ** (-0.5)
        q_t[h] = jnp.where(half_of == h % 2, pair, 0.0).astype(BF16)

    def attend(slot, p, own):
        gate = gates[slot].T
        for h in (2 * p, 2 * p + 1):
            s = dot(kv[slot, 2 * p], q_t[h]) - gate[:, h : h + 1]
            if own:
                s = jnp.where(iota((rows, rows), 0) <= iota((rows, rows), 1), s, -jnp.inf)
                top = jnp.max(s, axis=0, keepdims=True)
            else:
                top = jnp.maximum(m_s[h], jnp.max(s, axis=0, keepdims=True))
            weights = jnp.exp(s - top)
            total = jnp.sum(weights, axis=0, keepdims=True)
            v_t = jnp.concatenate(
                [
                    kv[slot, 2 * p + 1, pl.ds(i * LANES + (h % 2) * HEAD_DIM, HEAD_DIM), :]
                    for i in range(pieces)
                ],
                axis=1,
            )
            summed = dot(v_t, weights.astype(BF16))
            if own:
                l_s[h] = total
                acc[h] = summed
            else:
                fade = jnp.exp(m_s[h] - top)
                l_s[h] = l_s[h] * fade + total
                acc[h] = acc[h] * fade + summed
            m_s[h] = top

    for p in range(pairs):
        attend(sp, p, True)

    loads[7].wait()
    gate_out = dot(xn[...], wog_v[...])
    og[...] = gate_out / (1.0 + jnp.exp(-gate_out))

    for k in range(1, ny):
        other = (y + k) % ny
        pltpu.make_async_remote_copy(
            src_ref=st.at[other], dst_ref=st.at[other], send_sem=st_send.at[0],
            recv_sem=st_recv.at[other], device_id=(sp, partner), device_id_type=MESH,
        ).wait_recv()

    chain_copy = pltpu.make_async_remote_copy(
        src_ref=chain_out, dst_ref=chain_in, send_sem=chain_send, recv_sem=chain_recv,
        device_id=((sp + ny) % (nz * ny), tp), device_id_type=MESH,
    )

    def advance_chain():
        for j in range(rec_heads):
            rows_at = slice(j * STATE_ROWS, (j + 1) * STATE_ROWS)
            state = chain_in[rows_at, :].astype(F32)
            for k in range(ny):
                @pl.when(y == k)
                def _():
                    incoming[rows_at, :] = state.astype(BF16)

                base = j * st_rows
                decay = st[k, base + STATE_ROWS : base + st_rows, :].astype(F32)[0:1]
                state = state * decay + st[k, base : base + STATE_ROWS, :].astype(F32)
            chain_out[rows_at, :] = state.astype(BF16)

        @pl.when(z < nz - 1)
        def _():
            chain_copy.start()

    @pl.when(z == 0)
    def _():
        chain_in[...] = jnp.zeros_like(chain_in)
        advance_chain()

    def attend_beside(d):
        for k in range(1, ny):
            other = (y + k) % ny

            @pl.when((d > 0) | (other < y))
            def _():
                slot = (z - d) * ny + other
                for p in range(pairs):
                    wait_pieces(slot, pieces_of(p))
                    attend(slot, p, False)

    def step(d, carry):
        for p in range(pairs):
            @pl.when(d < z)
            def _():
                pass_on(z - d - 1, p)

            attend((z - d) * ny + y, p, False)

        @pl.when(d == jnp.maximum(z - 1, 1))
        def _():
            chain_copy.wait_recv()
            advance_chain()

        attend_beside(d - 1)
        return carry

    lax.fori_loop(1, z + 1, step, 0)
    for j in range(rec_heads):
        lanes = slice(j * STATE_ROWS, (j + 1) * STATE_ROWS)
        out = inner[:, lanes] + dot_nt(vq[:, lanes], incoming[lanes, :])
        mean = jnp.mean(out * out, axis=-1, keepdims=True)
        out = out * lax.rsqrt(mean + EPSILON) * r_gain[:, lanes] * og[:, lanes]
        vq[:, lanes] = out.astype(BF16)
    loads[9].wait()
    rec_part[...] = dot(vq[...], wro_v[...])

    attend_beside(z)

    for h in range(heads):
        mixed = acc[h] / l_s[h]
        mean = jnp.mean(mixed * mixed, axis=0, keepdims=True)
        attn_t[h * HEAD_DIM : (h + 1) * HEAD_DIM, :] = mixed * lax.rsqrt(mean + EPSILON)
        logsum_ref[h : h + 1, :] = m_s[h] + jnp.log(l_s[h]) + gate_t[h : h + 1, :]
    attn_out = (attn_t[...].T * a_gain[...]).astype(BF16)
    loads[8].wait()

    def rows_of(which_chip, which_core):
        return pl.ds(pl.multiple_of((which_chip * 2 + which_core) * rb, rb), rb)

    def columns(q):
        return slice(q * part_cols, (q + 1) * part_cols)

    def within(j, q):
        return pltpu.make_async_remote_copy(
            src_ref=part.at[q, rows_of(j, 1 - core)], dst_ref=recv1.at[j, q],
            send_sem=s1_send.at[j, q], recv_sem=s1_recv.at[j, q], device_id=(sp, partner),
            device_id_type=MESH,
        )

    def between(j, q):
        return pltpu.make_async_remote_copy(
            src_ref=send2.at[j, q], dst_ref=recv2.at[chip, q], send_sem=s2_send.at[j, q],
            recv_sem=s2_recv.at[chip, q], device_id=(sp, j * 2 + core), device_id_type=MESH,
        )

    order = [(chip + k) % chips for k in range(1, chips)]

    def chip_sum(j, q):
        within(j, q).wait_recv()
        return part[q, rows_of(j, core), :].astype(F32) + recv1[j, q].astype(F32)

    def send_sums(q):
        for j in order:
            send2[j, q] = chip_sum(j, q).astype(BF16)
            between(j, q).start()

    for q in range(splits):
        part[q] = (
            dot(attn_out, wao_v[:, columns(q)]) + rec_part[:, columns(q)]
        ).astype(BF16)
        for j in order:
            within(j, q).start()
        if q > 0:
            send_sums(q - 1)
    send_sums(splits - 1)
    for q in range(splits):
        within(chip, q).start()
    for q in range(splits):
        total = chip_sum(chip, q)
        for j in order:
            pltpu.make_async_remote_copy(
                src_ref=send2.at[j, q], dst_ref=recv2.at[j, q], send_sem=s2_send.at[j, q],
                recv_sem=s2_recv.at[j, q], device_id=(sp, partner), device_id_type=MESH,
            ).wait_recv()
            total = total + recv2[j, q].astype(F32)
        mixed_ref[:, columns(q)] = total.astype(BF16)

    for q in range(splits):
        for j in order + [chip]:
            within(j, q).wait_send()
        for j in order:
            between(j, q).wait_send()
    for k in range(1, ny):
        st_copy(k).wait_send()

        @pl.when(y + k < ny)
        def _():
            for i in every:
                side_copy(z, k, i).wait_send()

    @pl.when(z < nz - 1)
    def _():
        chain_copy.wait_send()
        for i in every:
            up_copy(z, i).wait_send()

    def drain(d, carry):
        source = z - d

        @pl.when(z < nz - 1)
        def _():
            for i in every:
                up_copy(source, i).wait_send()

        for k in range(1, ny):
            for i in every:
                side_copy(source, k, i).wait_send()
        return carry

    lax.fori_loop(1, z + 1, drain, 0)


def body(
    n_sp, n_tp,
    layer_input_rows, input_norm_gain, query_weight, key_weight, value_weight, query_norm_gain,
    key_norm_gain, cumulative_gate, attention_norm_gain, recurrence_query_weight, forget_weight,
    recurrence_value_weight, output_gate_weight, gate_lower_slack, extra_log_decay,
    recurrence_norm_gain, attention_output_weight, recurrence_output_weight,
):
    nz, ny = grid_of(n_sp)
    rows, width = layer_input_rows.shape
    cols = query_weight.shape[1]
    heads, pairs, rec_heads = cols // HEAD_DIM, cols // LANES, cols // STATE_ROWS
    rb, chips = rows // n_tp, n_tp // 2
    kinds, splits = 1 + 2 * pairs, math.gcd(width // LANES, 4)
    weight = pltpu.VMEM((width, cols), BF16)
    out_weight = pltpu.VMEM((cols, width), BF16)
    dma = pltpu.SemaphoreType.DMA
    any_space = pl.BlockSpec(memory_space=pl.ANY)
    vmem = pl.BlockSpec(memory_space=pltpu.VMEM)
    mixed, log_sum = pl.pallas_call(
        functools.partial(kernel, (nz, ny, n_tp)),
        name="mixer",
        out_shape=(
            jax.ShapeDtypeStruct((rb, width), BF16),
            jax.ShapeDtypeStruct((heads, rows), F32),
        ),
        in_specs=[any_space] * 18,
        out_specs=(vmem, vmem),
        scratch_shapes=[
            pltpu.VMEM((rows, width), BF16),
            *([weight] * 7), out_weight, out_weight,
            pltpu.VMEM((rows, width), BF16),
            pltpu.VMEM((n_sp, 2 * pairs, rows, LANES), BF16),
            pltpu.VMEM((n_sp, 8, rows), F32),
            pltpu.VMEM((heads, LANES, rows), BF16),
            pltpu.VMEM((heads, 1, rows), F32),
            pltpu.VMEM((heads, 1, rows), F32),
            pltpu.VMEM((heads, HEAD_DIM, rows), F32),
            pltpu.VMEM((cols, rows), F32),
            pltpu.VMEM((rows, cols), F32),
            pltpu.VMEM((rows, cols), BF16),
            pltpu.VMEM((rows, cols), F32),
            pltpu.VMEM((8, rows), F32),
            pltpu.VMEM((ny, rec_heads * (STATE_ROWS + 16), STATE_ROWS), BF16),
            pltpu.VMEM((cols, STATE_ROWS), BF16),
            pltpu.VMEM((cols, STATE_ROWS), BF16),
            pltpu.VMEM((cols, STATE_ROWS), BF16),
            pltpu.VMEM((splits, rows, width // splits), BF16),
            *([pltpu.VMEM((chips, splits, rb, width // splits), BF16)] * 3),
            *([pltpu.VMEM((1, n), F32) for n in (width, HEAD_DIM, HEAD_DIM)]),
            pltpu.VMEM((heads, rows), F32),
            pltpu.VMEM((1, cols), F32),
            pltpu.VMEM((1, cols), F32),
            pltpu.VMEM((rec_heads, rows), F32),
            pltpu.VMEM((1, cols), F32),
            pltpu.VMEM((rows, width), F32),
            dma((18,)),
            dma((nz, kinds)), dma((nz, ny, kinds)), dma((n_sp, kinds)),
            dma((ny,)), dma((ny,)), dma, dma,
            *([dma((chips, splits))] * 4),
        ],
        compiler_params=pltpu.CompilerParams(
            collective_id=0, has_side_effects=True, vmem_limit_bytes=60 * 1024 * 1024
        ),
    )(
        layer_input_rows, key_weight, value_weight, forget_weight, recurrence_value_weight,
        recurrence_query_weight, query_weight, output_gate_weight, attention_output_weight,
        recurrence_output_weight,
        input_norm_gain.reshape(1, -1), query_norm_gain.reshape(1, -1),
        key_norm_gain.reshape(1, -1), cumulative_gate.T, attention_norm_gain.reshape(1, -1),
        gate_lower_slack.reshape(1, -1), extra_log_decay.T, recurrence_norm_gain.reshape(1, -1),
    )
    return mixed, log_sum.T


def solution(mesh):
    return jax.shard_map(
        functools.partial(body, mesh.shape["sp"], mesh.shape["tp"]),
        mesh=mesh,
        in_specs=(
            P("sp", None),
            P(),
            P(None, "tp"),
            P(None, "tp"),
            P(None, "tp"),
            P(),
            P(),
            P("sp", "tp"),
            P("tp"),
            P(None, "tp"),
            P(None, "tp"),
            P(None, "tp"),
            P(None, "tp"),
            P("tp"),
            P("sp", "tp"),
            P("tp"),
            P("tp", None),
            P("tp", None),
        ),
        out_specs=(P(("sp", "tp"), None), P("sp", "tp")),
        check_vma=False,
    )
```

profile of v0, /device:TPU:25, one launch (start us, length us, event | category | flops | bytes accessed | tf_op | source)
XLA Modules:
  0.0 44.1 jit_solution(9758621611723256476)
XLA Ops:
  0.6 41.1 %mixer.1 = (bf16[64,2048]{1,0:T(8,128)(2,1)}, f32[4,256]{1,0:T(4,128)}) custom-call(bf16[256,2048]{1,0:T(8,128)(2,1)} %x_hbm.1, bf16[2048,256]{1,0:T(8,128)(2,1)} %wk_hbm.1, bf16[2048,256]{1,0:T(8,128)(2,1)} %wv_hbm.1, bf16[2048,256]{1,0:T(8,128)(2,1)} %wf_hbm.1, bf16[2048,256]{1,0:T(8,128)(2,1)} %wrv_hbm.1, bf16[2048,256]{1,0:T(8,128)(2,1)} %wrq_hbm.1, ...), custom_call_target="tpu_custom_call" | custom-call | tf_op jit(solution)/shard_map/mixer/pallas_call | solution.py:475
  41.8 0.0 copy-start
  41.8 1.7 %copy.22 = bf16[64,2048]{1,0:T(8,128)(2,1)} copy(bf16[64,2048]{1,0:T(8,128)(2,1)} %get-tuple-element.8) | data formatting | bytes 524288
  43.5 0.0 copy-done
  43.5 0.6 %copy.23 = f32[256,4]{0,1:T(4,128)} copy(f32[256,4]{0,1:T(4,128)S(1)} %bitcast.11) | data formatting | bytes 8192
Async XLA Ops:
  41.8 1.7 %copy-start = (f32[4,256]{1,0:T(4,128)S(1)}, f32[4,256]{1,0:T(4,128)}, u32[]{:S(2)}) copy-start(f32[4,256]{1,0:T(4,128)} %get-tuple-element.5) | copy-start | bytes 12292
where the time goes:
time: 44.4 us; the launch traced here: 44.1 us
  Pallas kernels  41.1 us (93%)
  local copies, waits for them, and re-layouts  2.27 us (5%)
  between operations  0.65 us (1%)
    pallas_call x1, Pallas kernels, body(): pl.pallas_call(functools.partial(kernel, (nz, ny, n_tp)), name='mixer', o...  41.1 us
    unnamed x4, local copies, waits for them, and re-layouts  2.27 us

commit v1 on v0

v1 whole, which is shorter than its diff:
```python
import functools
import math

import jax
import jax.numpy as jnp
from jax import lax
from jax.experimental import pallas as pl
from jax.experimental.pallas import tpu as pltpu
from jax.sharding import PartitionSpec as P

HEAD_DIM = 64
STATE_ROWS = 128
LANES = 128
EPSILON = 1e-06
MESH = pl.DeviceIdType.MESH
F32 = jnp.float32
BF16 = jnp.bfloat16


def dot(a, b):
    return jnp.dot(a, b, preferred_element_type=F32)


def parts_of(a, count):
    parts = []
    for _ in range(count):
        parts.append(a.astype(BF16))
        a = a - parts[-1].astype(F32)
    return parts


def dot_nt(a, b):
    return lax.dot_general(
        a, b, (((1,), (1,)), ((), ())), preferred_element_type=F32
    )


def iota(shape, axis):
    return lax.broadcasted_iota(jnp.int32, shape, axis)


def grid_of(count):
    columns = max(c for c in range(1, math.isqrt(count) + 1) if count % c == 0)
    return count // columns, columns


def kernel(
    sizes,
    x_hbm, wk_hbm, wv_hbm, wf_hbm, wrv_hbm, wrq_hbm, wq_hbm, wog_hbm, wao_hbm, wro_hbm,
    in_gain_hbm, q_gain_hbm, k_gain_hbm, gate_t_hbm, a_gain_hbm,
    slack_hbm, extra_t_hbm, r_gain_hbm,
    mixed_ref, logsum_ref,
    x_v, wkq_v, wvf_v, wrr_v, wog_v, wao_v, wro_v,
    xn, k_src, q_src, v_src, g_src, k_all, v_all, g_all, ga, q_in, s_buf, w_buf, m_s, l_s,
    o_src, lg_src, o_in, lg_in,
    inner, vq, og, ext, st, chain_in, chain_out, incoming, part, send2, recv1, recv2,
    in_gain, q_gain, k_gain, gate_t, a_gain, slack, extra_t, r_gain, rec_part,
    load_sem, k_send, v_send, q_send, g_send, k_recv, v_recv, q_recv, g_recv, k_fwd, v_fwd,
    o_send, o_recv, lg_send, lg_recv,
    st_send, st_recv, chain_send, chain_recv,
    s1_send, s1_recv, s2_send, s2_recv,
):
    nz, ny, ntp = sizes
    n_sp = nz * ny
    rows, width = x_v.shape
    cols = wog_v.shape[1]
    heads = cols // HEAD_DIM
    pairs = cols // LANES
    rec_heads = cols // STATE_ROWS
    chips = ntp // 2
    rb = rows // ntp
    half = rows // 2
    splits = s1_send.shape[1]
    part_cols = width // splits
    homes = n_sp // (2 * heads)
    members = 2 * homes

    sp, tp = lax.axis_index("sp"), lax.axis_index("tp")
    z, y = sp // ny, sp % ny
    chip, core = tp // 2, tp % 2
    partner = chip * 2 + (1 - core)

    group = sp // homes
    src_core, src_head = group % 2, group // 2
    primary = core == src_core
    member = (sp % homes) * 2 + core
    src_tp = chip * 2 + src_core

    def block_of(j):
        return j * members + (member if j % 2 == 0 else members - 1 - member)

    my_j = sp // members
    my_u = sp % members
    my_member = my_u + (my_j % 2) * (members - 1 - 2 * my_u)
    my_home, my_core = my_member // 2, my_member % 2

    def home_of(i, r):
        return (2 * i + core) * homes + r

    loads = []
    for i, (src, dst) in enumerate((
        (x_hbm, x_v), (wk_hbm, wkq_v.at[:, 0:cols]), (wq_hbm, wkq_v.at[:, cols : 2 * cols]),
        (wv_hbm, wvf_v.at[:, 0:cols]), (wf_hbm, wvf_v.at[:, cols : 2 * cols]),
        (wrv_hbm, wrr_v.at[:, 0:cols]), (wrq_hbm, wrr_v.at[:, cols : 2 * cols]),
        (wog_hbm, wog_v), (wao_hbm, wao_v), (wro_hbm, wro_v),
        (in_gain_hbm, in_gain), (q_gain_hbm, q_gain), (k_gain_hbm, k_gain),
        (gate_t_hbm, gate_t), (a_gain_hbm, a_gain), (slack_hbm, slack),
        (extra_t_hbm, extra_t), (r_gain_hbm, r_gain),
    )):
        loads.append(pltpu.make_async_copy(src, dst, load_sem.at[i]))

    for copy in loads[:1] + loads[10:] + loads[1:3]:
        copy.start()

    barrier = pltpu.get_barrier_semaphore()

    def greet(where):
        pl.semaphore_signal(barrier, inc=1, device_id=where, device_id_type=MESH)

    for k in range(n_sp):
        if k > 0:
            greet(((sp + k) % n_sp, tp))
        greet(((sp + k) % n_sp, partner))
    for k in range(1, chips):
        greet((sp, ((chip + k) % chips) * 2 + core))

    loads[0].wait()
    for copy in loads[10:]:
        copy.wait()
    for copy in loads[3:5]:
        copy.start()
    xf = x_v[...].astype(F32)
    scale = lax.rsqrt(jnp.mean(xf * xf, axis=-1, keepdims=True) + EPSILON)
    xn[...] = (xf * scale * in_gain[...]).astype(BF16)

    for i in range(heads):
        g_src[i] = gate_t[i : i + 1, :]

    block_ones = jnp.where(
        iota((cols, cols), 0) // HEAD_DIM == iota((cols, cols), 1) // HEAD_DIM, 1.0 / HEAD_DIM, 0.0
    ).astype(BF16)

    def head_norm(v, gain_ref):
        mean = sum(dot(p, block_ones) for p in parts_of(v * v, 2))
        gain = jnp.concatenate([gain_ref[...]] * heads, axis=1)
        return v * lax.rsqrt(mean + EPSILON) * gain

    loads[1].wait()
    loads[2].wait()
    for copy in loads[5:7]:
        copy.start()
    kq = dot(xn[...], wkq_v[...])
    keys = head_norm(kq[:, 0:cols], k_gain)
    first_half = iota((half, LANES), 1) < HEAD_DIM
    for p in range(pairs):
        low = keys[0:half, p * LANES : (p + 1) * LANES]
        high = keys[half:rows, p * LANES : (p + 1) * LANES]
        k_src[2 * p] = jnp.where(first_half, low, pltpu.roll(high, HEAD_DIM, 1)).astype(BF16)
        k_src[2 * p + 1] = jnp.where(first_half, pltpu.roll(low, HEAD_DIM, 1), high).astype(BF16)
    queries_t = (head_norm(kq[:, cols : 2 * cols], q_gain).astype(BF16).astype(F32)).T
    for i in range(heads):
        q_src[i] = (queries_t[i * HEAD_DIM : (i + 1) * HEAD_DIM, :] * HEAD_DIM ** (-0.5)).astype(BF16)

    greeted = 2 * n_sp - 1 + chips - 1
    pl.semaphore_wait(barrier, greeted)

    def remote(src, dst, send, recv, where):
        return pltpu.make_async_remote_copy(
            src_ref=src, dst_ref=dst, send_sem=send, recv_sem=recv,
            device_id=where, device_id_type=MESH,
        )

    def k_copy(i, r):
        return remote(
            k_src.at[i], k_all.at[sp], k_send.at[i, r], k_recv.at[sp], (home_of(i, r), tp)
        )

    def v_copy(i, r):
        return remote(
            v_src.at[i], v_all.at[sp], v_send.at[i, r], v_recv.at[sp], (home_of(i, r), tp)
        )

    def g_copy(i, r, c):
        return remote(
            g_src.at[i], g_all.at[sp], g_send.at[i, r, c], g_recv.at[sp],
            (home_of(i, r), tp if c == 0 else partner),
        )

    def q_copy(i):
        return remote(
            q_src.at[i], q_in.at[my_j], q_send.at[i], q_recv.at[my_j],
            (home_of(i, my_home), chip * 2 + my_core),
        )

    def spread(copies, local):
        for i in range(heads):
            for r in range(homes):
                @pl.when(home_of(i, r) != sp)
                def _():
                    copies(i, r).start()

                @pl.when(home_of(i, r) == sp)
                def _():
                    local(i)

    def keep_k(i):
        k_all[sp] = k_src[i]

    def keep_v(i):
        v_all[sp] = v_src[i]

    def keep_g(i):
        g_all[sp] = g_src[i]

    spread(k_copy, keep_k)
    for i in range(heads):
        stays = (home_of(i, my_home) == sp) & (my_core == core)

        @pl.when(jnp.logical_not(stays))
        def _():
            q_copy(i).start()

        @pl.when(stays)
        def _():
            q_in[my_j] = q_src[i]
    spread(lambda i, r: g_copy(i, r, 0), keep_g)
    for i in range(heads):
        for r in range(homes):
            g_copy(i, r, 1).start()

    loads[3].wait()
    loads[4].wait()
    for copy in loads[7:10]:
        copy.start()
    vf = dot(xn[...], wvf_v[...])
    values_t = vf[:, 0:cols].T.astype(BF16)
    for i in range(heads):
        v_src[i] = values_t[i * HEAD_DIM : (i + 1) * HEAD_DIM, :]
    spread(v_copy, keep_v)

    tri = iota((rows, rows), 0) >= iota((rows, rows), 1)
    tri_b = tri.astype(F32).astype(BF16)
    share = slack[...] / (1.0 + jnp.exp(vf[:, cols : 2 * cols]))
    run = sum(dot(tri_b, p) for p in parts_of(jnp.log1p(-share), 3))
    ext[...] = jnp.zeros_like(ext)
    ext[0:rec_heads, :] = extra_t[...]
    ext_row = sum(dot_nt(p, tri_b) for p in parts_of(ext[...], 3))
    ext_col = ext_row.T
    loads[5].wait()
    loads[6].wait()
    rr = dot(xn[...], wrr_v[...])
    rec_value = rr[:, 0:cols]
    rec_query = rr[:, cols : 2 * cols]
    rec_query = rec_query / (1.0 + jnp.exp(-rec_query))
    last = run[rows - 1 : rows]
    st_rows = STATE_ROWS + 16
    for j in range(rec_heads):
        lanes = slice(j * STATE_ROWS, (j + 1) * STATE_ROWS)
        e_col = ext_col[:, j : j + 1]
        e_row = ext_row[j : j + 1, :]
        e_last = e_row[:, rows - 1 : rows]
        left = share[:, lanes] * jnp.exp(last[:, lanes] - run[:, lanes] + (e_last - e_col))
        st[y, j * st_rows : j * st_rows + STATE_ROWS, :] = dot(
            rec_value[:, lanes].T.astype(BF16), left.astype(BF16)
        ).astype(BF16)
        st[y, j * st_rows + STATE_ROWS : (j + 1) * st_rows, :] = jnp.broadcast_to(
            jnp.exp(last[:, lanes] + e_last), (16, STATE_ROWS)
        ).astype(BF16)

    def st_copy(k):
        return remote(
            st.at[y], st.at[y], st_send.at[k], st_recv.at[y], (z * ny + (y + k) % ny, tp)
        )

    for k in range(1, ny):
        st_copy(k).start()

    grown = rec_query * jnp.exp(run)
    for j in range(rec_heads):
        lanes = slice(j * STATE_ROWS, (j + 1) * STATE_ROWS)
        e_col = ext_col[:, j : j + 1]
        e_row = ext_row[j : j + 1, :]
        value = rec_value[:, lanes].astype(BF16)
        scores = dot_nt(
            grown[:, lanes].astype(BF16), (share[:, lanes] * jnp.exp(-run[:, lanes])).astype(BF16)
        )
        fading = jnp.exp(jnp.where(tri, e_col - e_row, -jnp.inf))
        scores = jnp.where(tri, scores * fading, 0.0)
        inner[:, lanes] = dot(scores.astype(BF16), value)
        vq[:, lanes] = (grown[:, lanes] * jnp.exp(e_col)).astype(BF16)

    chain_copy = remote(
        chain_out, chain_in, chain_send, chain_recv, ((sp + ny) % n_sp, tp)
    )

    for k in range(1, ny):
        other = (y + k) % ny
        remote(
            st.at[other], st.at[other], st_send.at[0], st_recv.at[other], (sp, partner)
        ).wait_recv()

    def advance_chain():
        for j in range(rec_heads):
            rows_at = slice(j * STATE_ROWS, (j + 1) * STATE_ROWS)
            state = chain_in[rows_at, :].astype(F32)
            for k in range(ny):
                @pl.when(y == k)
                def _():
                    incoming[rows_at, :] = state.astype(BF16)

                base = j * st_rows
                decay = st[k, base + STATE_ROWS : base + st_rows, :].astype(F32)[0:1]
                state = state * decay + st[k, base : base + STATE_ROWS, :].astype(F32)
            chain_out[rows_at, :] = state.astype(BF16)

        @pl.when(z < nz - 1)
        def _():
            chain_copy.start()

    @pl.when(z == 0)
    def _():
        chain_in[...] = jnp.zeros_like(chain_in)
        advance_chain()

    def chain_at(here):
        @pl.when(here)
        def _():
            chain_copy.wait_recv()
            advance_chain()

    loads[7].wait()
    gate_out = dot(xn[...], wog_v[...])
    og[...] = gate_out / (1.0 + jnp.exp(-gate_out))

    for t in range(n_sp):
        @pl.when((sp != t) | jnp.logical_not(primary))
        def _():
            remote(
                g_all.at[t], g_all.at[t], g_send.at[0, 0, 0], g_recv.at[t], (sp, partner)
            ).wait_recv()

    gate_cols = jnp.concatenate(
        [g_all[t, :, h * half : (h + 1) * half] for t in range(n_sp) for h in range(2)], axis=0
    ).T
    gate_parts = jnp.concatenate(
        [p.astype(F32) for p in parts_of(gate_cols, 3)]
        + [jnp.zeros((half, LANES - 6 * n_sp), F32)] * (6 * n_sp < LANES), axis=1
    )
    lane_block = (iota((half, LANES), 1) % (2 * n_sp)) // 2
    for t in range(n_sp):
        ga[t] = jnp.where(lane_block == t, gate_parts, 0.0).astype(BF16)

    def wait_all(ref, fwd, recv):
        for t in range(n_sp):
            copy = remote(ref.at[t], ref.at[t], fwd.at[t], recv.at[t], (sp, partner))

            @pl.when((sp != t) | jnp.logical_not(primary))
            def _():
                copy.wait_recv()

            @pl.when(primary)
            def _():
                copy.start()

    chain_at(z == 1)
    wait_all(k_all, k_fwd, k_recv)
    chain_at(z == 2)

    minus = jnp.where(
        iota((LANES, 2 * rows), 0) % 2 == iota((LANES, 2 * rows), 1) // rows, -1.0, 0.0
    ).astype(BF16)
    ahead = (
        iota((half, 2 * rows), 0) + half * (iota((half, 2 * rows), 1) // rows)
        - iota((half, 2 * rows), 1) % rows
    )
    first = [members * j * (j + 1) // 2 for j in range(heads)]

    def weigh(j):
        remote(
            q_in.at[j], q_in.at[j], q_send.at[0], q_recv.at[j], (sp, partner)
        )
        kept = (block_of(j) == sp) & primary

        @pl.when(jnp.logical_not(kept))
        def _():
            remote(
                q_in.at[j], q_in.at[j], q_send.at[0], q_recv.at[j], (sp, partner)
            ).wait_recv()

        q = q_in[j]
        none = jnp.zeros_like(q)
        right = jnp.concatenate(
            [jnp.concatenate([q, none], axis=1), jnp.concatenate([none, q], axis=1), minus], axis=0
        )
        top = None
        for t in range((j + 1) * members):
            s = dot(jnp.concatenate([k_all[t], ga[t]], axis=1), right)
            if t >= j * members:
                s = jnp.where(ahead <= (block_of(j) - t) * rows, s, -jnp.inf)
            s_buf[t] = s
            here = jnp.max(s, axis=0, keepdims=True)
            top = here if top is None else jnp.maximum(top, here)
        top = jnp.maximum(top[:, 0:rows], top[:, rows : 2 * rows])
        m_s[j] = top
        top = jnp.concatenate([top, top], axis=1)
        total = None
        for t in range((j + 1) * members):
            w = jnp.exp(s_buf[t] - top)
            here = jnp.sum(w, axis=0, keepdims=True)
            total = here if total is None else total + here
            w = w.astype(BF16)
            w_buf[first[j] + t, 0:half, :] = w[:, 0:rows]
            w_buf[first[j] + t, half:rows, :] = w[:, rows : 2 * rows]
        l_s[j] = total[:, 0:rows] + total[:, rows : 2 * rows]

    def o_copy(j):
        return remote(
            o_src.at[j], o_in.at[src_head], o_send.at[j], o_recv.at[src_head],
            (block_of(j), src_tp),
        )

    def lg_copy(j):
        return remote(
            lg_src.at[j], lg_in.at[src_head], lg_send.at[j], lg_recv.at[src_head],
            (block_of(j), src_tp),
        )

    def finish(j):
        n = (j + 1) * members
        summed = [
            sum(dot(v_all[t], w_buf[first[j] + t]) for t in range(u, n, 2)) for u in range(2)
        ]
        out = (summed[0] + summed[1]) / l_s[j]
        mean = jnp.mean(out * out, axis=0, keepdims=True)
        o_src[j] = (out * lax.rsqrt(mean + EPSILON)).astype(BF16)
        lg_src[j] = m_s[j] + jnp.log(l_s[j])
        kept = (block_of(j) == sp) & primary

        @pl.when(jnp.logical_not(kept))
        def _():
            o_copy(j).start()
            lg_copy(j).start()

        @pl.when(kept)
        def _():
            o_in[src_head] = o_src[j]
            lg_in[src_head] = lg_src[j]

    for j in range(heads):
        weigh(j)
    wait_all(v_all, v_fwd, v_recv)
    for j in range(heads):
        finish(j)

    chain_at(z >= 3)
    for j in range(rec_heads):
        lanes = slice(j * STATE_ROWS, (j + 1) * STATE_ROWS)
        out = inner[:, lanes] + dot_nt(vq[:, lanes], incoming[lanes, :])
        mean = jnp.mean(out * out, axis=-1, keepdims=True)
        out = out * lax.rsqrt(mean + EPSILON) * r_gain[:, lanes] * og[:, lanes]
        vq[:, lanes] = out.astype(BF16)
    loads[9].wait()
    rec_part[...] = dot(vq[...], wro_v[...])
    loads[8].wait()

    for i in range(heads):
        kept = (home_of(i, my_home) == sp) & (my_core == core)

        @pl.when(jnp.logical_not(kept))
        def _():
            remote(
                o_in.at[i], o_in.at[i], o_send.at[0], o_recv.at[i], (sp, partner)
            ).wait_recv()
            remote(
                lg_in.at[i], lg_in.at[i], lg_send.at[0], lg_recv.at[i], (sp, partner)
            ).wait_recv()

    for i in range(heads):
        logsum_ref[i : i + 1, :] = lg_in[i] + gate_t[i : i + 1, :]
    attn_t = jnp.concatenate([o_in[i].astype(F32) for i in range(heads)], axis=0)
    attn_out = (attn_t.T * a_gain[...]).astype(BF16)

    def rows_of(which_chip, which_core):
        return pl.ds(pl.multiple_of((which_chip * 2 + which_core) * rb, rb), rb)

    def columns(q):
        return slice(q * part_cols, (q + 1) * part_cols)

    def within(j, q):
        return pltpu.make_async_remote_copy(
            src_ref=part.at[q, rows_of(j, 1 - core)], dst_ref=recv1.at[j, q],
            send_sem=s1_send.at[j, q], recv_sem=s1_recv.at[j, q], device_id=(sp, partner),
            device_id_type=MESH,
        )

    def between(j, q):
        return pltpu.make_async_remote_copy(
            src_ref=send2.at[j, q], dst_ref=recv2.at[chip, q], send_sem=s2_send.at[j, q],
            recv_sem=s2_recv.at[chip, q], device_id=(sp, j * 2 + core), device_id_type=MESH,
        )

    order = [(chip + k) % chips for k in range(1, chips)]

    def chip_sum(j, q):
        within(j, q).wait_recv()
        return part[q, rows_of(j, core), :].astype(F32) + recv1[j, q].astype(F32)

    def send_sums(q):
        for j in order:
            send2[j, q] = chip_sum(j, q).astype(BF16)
            between(j, q).start()

    for q in range(splits):
        part[q] = (
            dot(attn_out, wao_v[:, columns(q)]) + rec_part[:, columns(q)]
        ).astype(BF16)
        for j in order:
            within(j, q).start()
        if q > 0:
            send_sums(q - 1)
    send_sums(splits - 1)
    for q in range(splits):
        within(chip, q).start()
    for q in range(splits):
        total = chip_sum(chip, q)
        for j in order:
            pltpu.make_async_remote_copy(
                src_ref=send2.at[j, q], dst_ref=recv2.at[j, q], send_sem=s2_send.at[j, q],
                recv_sem=s2_recv.at[j, q], device_id=(sp, partner), device_id_type=MESH,
            ).wait_recv()
            total = total + recv2[j, q].astype(F32)
        mixed_ref[:, columns(q)] = total.astype(BF16)

    for q in range(splits):
        for j in order + [chip]:
            within(j, q).wait_send()
        for j in order:
            between(j, q).wait_send()
    for k in range(1, ny):
        st_copy(k).wait_send()

    @pl.when(z < nz - 1)
    def _():
        chain_copy.wait_send()

    for i in range(heads):
        for r in range(homes):
            @pl.when(home_of(i, r) != sp)
            def _():
                k_copy(i, r).wait_send()
                v_copy(i, r).wait_send()
                g_copy(i, r, 0).wait_send()

            g_copy(i, r, 1).wait_send()

        @pl.when((home_of(i, my_home) != sp) | (my_core != core))
        def _():
            q_copy(i).wait_send()

    @pl.when(primary)
    def _():
        for t in range(n_sp):
            remote(k_all.at[t], k_all.at[t], k_fwd.at[t], k_recv.at[t], (sp, partner)).wait_send()
            remote(v_all.at[t], v_all.at[t], v_fwd.at[t], v_recv.at[t], (sp, partner)).wait_send()

    for j in range(heads):
        @pl.when((block_of(j) != sp) | jnp.logical_not(primary))
        def _():
            o_copy(j).wait_send()
            lg_copy(j).wait_send()


def body(
    n_sp, n_tp,
    layer_input_rows, input_norm_gain, query_weight, key_weight, value_weight, query_norm_gain,
    key_norm_gain, cumulative_gate, attention_norm_gain, recurrence_query_weight, forget_weight,
    recurrence_value_weight, output_gate_weight, gate_lower_slack, extra_log_decay,
    recurrence_norm_gain, attention_output_weight, recurrence_output_weight,
):
    nz, ny = grid_of(n_sp)
    rows, width = layer_input_rows.shape
    cols = query_weight.shape[1]
    heads, pairs, rec_heads = cols // HEAD_DIM, cols // LANES, cols // STATE_ROWS
    rb, chips = rows // n_tp, n_tp // 2
    half = rows // 2
    homes = n_sp // (2 * heads)
    blocks = 2 * homes * heads * (heads + 1) // 2
    splits = math.gcd(width // LANES, 4)
    weight = pltpu.VMEM((width, cols), BF16)
    two_weights = pltpu.VMEM((width, 2 * cols), BF16)
    out_weight = pltpu.VMEM((cols, width), BF16)
    dma = pltpu.SemaphoreType.DMA
    any_space = pl.BlockSpec(memory_space=pl.ANY)
    vmem = pl.BlockSpec(memory_space=pltpu.VMEM)
    mixed, log_sum = pl.pallas_call(
        functools.partial(kernel, (nz, ny, n_tp)),
        name="mixer",
        out_shape=(
            jax.ShapeDtypeStruct((rb, width), BF16),
            jax.ShapeDtypeStruct((heads, rows), F32),
        ),
        in_specs=[any_space] * 18,
        out_specs=(vmem, vmem),
        scratch_shapes=[
            pltpu.VMEM((rows, width), BF16),
            *([two_weights] * 3), weight, out_weight, out_weight,
            pltpu.VMEM((rows, width), BF16),
            pltpu.VMEM((heads, half, LANES), BF16),
            pltpu.VMEM((heads, HEAD_DIM, rows), BF16),
            pltpu.VMEM((heads, HEAD_DIM, rows), BF16),
            pltpu.VMEM((heads, 1, rows), F32),
            pltpu.VMEM((n_sp, half, LANES), BF16),
            pltpu.VMEM((n_sp, HEAD_DIM, rows), BF16),
            pltpu.VMEM((n_sp, 1, rows), F32),
            pltpu.VMEM((n_sp, half, LANES), BF16),
            pltpu.VMEM((heads, HEAD_DIM, rows), BF16),
            pltpu.VMEM((n_sp, half, 2 * rows), F32),
            pltpu.VMEM((blocks, rows, rows), BF16),
            pltpu.VMEM((heads, 1, rows), F32),
            pltpu.VMEM((heads, 1, rows), F32),
            pltpu.VMEM((heads, HEAD_DIM, rows), BF16),
            pltpu.VMEM((heads, 1, rows), F32),
            pltpu.VMEM((heads, HEAD_DIM, rows), BF16),
            pltpu.VMEM((heads, 1, rows), F32),
            pltpu.VMEM((rows, cols), F32),
            pltpu.VMEM((rows, cols), BF16),
            pltpu.VMEM((rows, cols), F32),
            pltpu.VMEM((8, rows), F32),
            pltpu.VMEM((ny, rec_heads * (STATE_ROWS + 16), STATE_ROWS), BF16),
            pltpu.VMEM((cols, STATE_ROWS), BF16),
            pltpu.VMEM((cols, STATE_ROWS), BF16),
            pltpu.VMEM((cols, STATE_ROWS), BF16),
            pltpu.VMEM((splits, rows, width // splits), BF16),
            *([pltpu.VMEM((chips, splits, rb, width // splits), BF16)] * 3),
            *([pltpu.VMEM((1, n), F32) for n in (width, HEAD_DIM, HEAD_DIM)]),
            pltpu.VMEM((heads, rows), F32),
            pltpu.VMEM((1, cols), F32),
            pltpu.VMEM((1, cols), F32),
            pltpu.VMEM((rec_heads, rows), F32),
            pltpu.VMEM((1, cols), F32),
            pltpu.VMEM((rows, width), F32),
            dma((18,)),
            dma((heads, homes)), dma((heads, homes)), dma((heads,)), dma((heads, homes, 2)),
            dma((n_sp,)), dma((n_sp,)), dma((heads,)), dma((n_sp,)), dma((n_sp,)), dma((n_sp,)),
            *([dma((heads,))] * 4),
            dma((ny,)), dma((ny,)), dma, dma,
            *([dma((chips, splits))] * 4),
        ],
        compiler_params=pltpu.CompilerParams(
            collective_id=0, has_side_effects=True, vmem_limit_bytes=60 * 1024 * 1024
        ),
    )(
        layer_input_rows, key_weight, value_weight, forget_weight, recurrence_value_weight,
        recurrence_query_weight, query_weight, output_gate_weight, attention_output_weight,
        recurrence_output_weight,
        input_norm_gain.reshape(1, -1), query_norm_gain.reshape(1, -1),
        key_norm_gain.reshape(1, -1), cumulative_gate.T, attention_norm_gain.reshape(1, -1),
        gate_lower_slack.reshape(1, -1), extra_log_decay.T, recurrence_norm_gain.reshape(1, -1),
    )
    return mixed, log_sum.T


def solution(mesh):
    return jax.shard_map(
        functools.partial(body, mesh.shape["sp"], mesh.shape["tp"]),
        mesh=mesh,
        in_specs=(
            P("sp", None),
            P(),
            P(None, "tp"),
            P(None, "tp"),
            P(None, "tp"),
            P(),
            P(),
            P("sp", "tp"),
            P("tp"),
            P(None, "tp"),
            P(None, "tp"),
            P(None, "tp"),
            P(None, "tp"),
            P("tp"),
            P("sp", "tp"),
            P("tp"),
            P("tp", None),
            P("tp", None),
        ),
        out_specs=(P(("sp", "tp"), None), P("sp", "tp")),
        check_vma=False,
    )
```

time: 44.4 us -> 40.7 us (0.917)
  the two profiles are of different devices: /device:TPU:25 before, /device:TPU:0 now
where the time goes in v1:
time: 40.7 us; the launch traced here: 40.6 us
  Pallas kernels  37.6 us (92%)
  local copies, waits for them, and re-layouts  2.27 us (6%)
  between operations  0.65 us (2%)
    pallas_call x1, Pallas kernels, body(): pl.pallas_call(functools.partial(kernel, (nz, ny, n_tp)), name='mixer', o...  37.6 us
    unnamed x4, local copies, waits for them, and re-layouts  2.27 us

profile of v1, /device:TPU:0, one launch (start us, length us, event | category | flops | bytes accessed | tf_op | source)
XLA Modules:
  0.0 40.6 jit_solution(9100632644429615440)
XLA Ops:
  0.6 37.6 %mixer.1 = (bf16[64,2048]{1,0:T(8,128)(2,1)}, f32[4,256]{1,0:T(4,128)}) custom-call(bf16[256,2048]{1,0:T(8,128)(2,1)} %x_hbm.1, bf16[2048,256]{1,0:T(8,128)(2,1)} %wk_hbm.1, bf16[2048,256]{1,0:T(8,128)(2,1)} %wv_hbm.1, bf16[2048,256]{1,0:T(8,128)(2,1)} %wf_hbm.1, bf16[2048,256]{1,0:T(8,128)(2,1)} %wrv_hbm.1, bf16[2048,256]{1,0:T(8,128)(2,1)} %wrq_hbm.1, ...), custom_call_target="tpu_custom_call" | custom-call | tf_op jit(solution)/shard_map/mixer/pallas_call | solution.py:595
  38.3 0.0 copy-start
  38.3 1.7 %copy.22 = bf16[64,2048]{1,0:T(8,128)(2,1)} copy(bf16[64,2048]{1,0:T(8,128)(2,1)} %get-tuple-element.8) | data formatting | bytes 524288
  40.0 0.0 copy-done
  40.0 0.6 %copy.23 = f32[256,4]{0,1:T(4,128)} copy(f32[256,4]{0,1:T(4,128)S(1)} %bitcast.11) | data formatting | bytes 8192
Async XLA Ops:
  38.3 1.7 %copy-start = (f32[4,256]{1,0:T(4,128)S(1)}, f32[4,256]{1,0:T(4,128)}, u32[]{:S(2)}) copy-start(f32[4,256]{1,0:T(4,128)} %get-tuple-element.5) | copy-start | bytes 12292

commit v2 on v1

--- a/solution.py
+++ b/solution.py
@@ -50,7 +50,7 @@
     in_gain_hbm, q_gain_hbm, k_gain_hbm, gate_t_hbm, a_gain_hbm,
     slack_hbm, extra_t_hbm, r_gain_hbm,
     mixed_ref, logsum_ref,
-    x_v, wkq_v, wvf_v, wrr_v, wog_v, wao_v, wro_v,
+    x_v, wkq_v, wfr_v, wvr_v, wog_v, wao_v, wro_v,
     xn, k_src, q_src, v_src, g_src, k_all, v_all, g_all, ga, q_in, s_buf, w_buf, m_s, l_s,
     o_src, lg_src, o_in, lg_in,
     inner, vq, og, ext, st, chain_in, chain_out, incoming, part, send2, recv1, recv2,
@@ -100,8 +100,8 @@
     loads = []
     for i, (src, dst) in enumerate((
         (x_hbm, x_v), (wk_hbm, wkq_v.at[:, 0:cols]), (wq_hbm, wkq_v.at[:, cols : 2 * cols]),
-        (wv_hbm, wvf_v.at[:, 0:cols]), (wf_hbm, wvf_v.at[:, cols : 2 * cols]),
-        (wrv_hbm, wrr_v.at[:, 0:cols]), (wrq_hbm, wrr_v.at[:, cols : 2 * cols]),
+        (wf_hbm, wfr_v.at[:, 0:cols]), (wrv_hbm, wfr_v.at[:, cols : 2 * cols]),
+        (wv_hbm, wvr_v.at[:, 0:cols]), (wrq_hbm, wvr_v.at[:, cols : 2 * cols]),
         (wog_hbm, wog_v), (wao_hbm, wao_v), (wro_hbm, wro_v),
         (in_gain_hbm, in_gain), (q_gain_hbm, q_gain), (k_gain_hbm, k_gain),
         (gate_t_hbm, gate_t), (a_gain_hbm, a_gain), (slack_hbm, slack),
@@ -161,9 +161,6 @@
     for i in range(heads):
         q_src[i] = (queries_t[i * HEAD_DIM : (i + 1) * HEAD_DIM, :] * HEAD_DIM ** (-0.5)).astype(BF16)
 
-    greeted = 2 * n_sp - 1 + chips - 1
-    pl.semaphore_wait(barrier, greeted)
-
     def remote(src, dst, send, recv, where):
         return pltpu.make_async_remote_copy(
             src_ref=src, dst_ref=dst, send_sem=send, recv_sem=recv,
@@ -192,8 +189,10 @@
             (home_of(i, my_home), chip * 2 + my_core),
         )
 
+    turns = [(src_head + k) % heads for k in range(heads)]
+
     def spread(copies, local):
-        for i in range(heads):
+        for i in turns:
             for r in range(homes):
                 @pl.when(home_of(i, r) != sp)
                 def _():
@@ -212,46 +211,47 @@
     def keep_g(i):
         g_all[sp] = g_src[i]
 
-    spread(k_copy, keep_k)
-    for i in range(heads):
-        stays = (home_of(i, my_home) == sp) & (my_core == core)
-
-        @pl.when(jnp.logical_not(stays))
-        def _():
-            q_copy(i).start()
-
-        @pl.when(stays)
-        def _():
-            q_in[my_j] = q_src[i]
-    spread(lambda i, r: g_copy(i, r, 0), keep_g)
-    for i in range(heads):
-        for r in range(homes):
-            g_copy(i, r, 1).start()
-
+    def begin():
+        pl.semaphore_wait(barrier, 2 * n_sp - 1 + chips - 1)
+
+    def send_keys_and_queries():
+        spread(lambda i, r: g_copy(i, r, 0), keep_g)
+        for i in range(heads):
+            for r in range(homes):
+                g_copy(i, r, 1).start()
+        spread(k_copy, keep_k)
+        for i in turns:
+            stays = (home_of(i, my_home) == sp) & (my_core == core)
+
+            @pl.when(jnp.logical_not(stays))
+            def _():
+                q_copy(i).start()
+
+            @pl.when(stays)
+            def _():
+                q_in[my_j] = q_src[i]
+
+    early = z == 0
+
+    @pl.when(jnp.logical_not(early))
+    def _():
+        begin()
+        send_keys_and_queries()
+
+    tri = iota((rows, rows), 0) >= iota((rows, rows), 1)
+    tri_b = tri.astype(F32).astype(BF16)
     loads[3].wait()
     loads[4].wait()
     for copy in loads[7:10]:
         copy.start()
-    vf = dot(xn[...], wvf_v[...])
-    values_t = vf[:, 0:cols].T.astype(BF16)
-    for i in range(heads):
-        v_src[i] = values_t[i * HEAD_DIM : (i + 1) * HEAD_DIM, :]
-    spread(v_copy, keep_v)
-
-    tri = iota((rows, rows), 0) >= iota((rows, rows), 1)
-    tri_b = tri.astype(F32).astype(BF16)
-    share = slack[...] / (1.0 + jnp.exp(vf[:, cols : 2 * cols]))
+    fr = dot(xn[...], wfr_v[...])
+    share = slack[...] / (1.0 + jnp.exp(fr[:, 0:cols]))
+    rec_value = fr[:, cols : 2 * cols]
     run = sum(dot(tri_b, p) for p in parts_of(jnp.log1p(-share), 3))
     ext[...] = jnp.zeros_like(ext)
     ext[0:rec_heads, :] = extra_t[...]
     ext_row = sum(dot_nt(p, tri_b) for p in parts_of(ext[...], 3))
     ext_col = ext_row.T
-    loads[5].wait()
-    loads[6].wait()
-    rr = dot(xn[...], wrr_v[...])
-    rec_value = rr[:, 0:cols]
-    rec_query = rr[:, cols : 2 * cols]
-    rec_query = rec_query / (1.0 + jnp.exp(-rec_query))
     last = run[rows - 1 : rows]
     st_rows = STATE_ROWS + 16
     for j in range(rec_heads):
@@ -272,9 +272,27 @@
             st.at[y], st.at[y], st_send.at[k], st_recv.at[y], (z * ny + (y + k) % ny, tp)
         )
 
+    @pl.when(early)
+    def _():
+        begin()
+
     for k in range(1, ny):
         st_copy(k).start()
 
+    @pl.when(early)
+    def _():
+        send_keys_and_queries()
+
+    loads[5].wait()
+    loads[6].wait()
+    vr = dot(xn[...], wvr_v[...])
+    values_t = vr[:, 0:cols].T.astype(BF16)
+    for i in range(heads):
+        v_src[i] = values_t[i * HEAD_DIM : (i + 1) * HEAD_DIM, :]
+    spread(v_copy, keep_v)
+
+    rec_query = vr[:, cols : 2 * cols]
+    rec_query = rec_query / (1.0 + jnp.exp(-rec_query))
     grown = rec_query * jnp.exp(run)
     for j in range(rec_heads):
         lanes = slice(j * STATE_ROWS, (j + 1) * STATE_ROWS)
@@ -289,9 +307,9 @@
         inner[:, lanes] = dot(scores.astype(BF16), value)
         vq[:, lanes] = (grown[:, lanes] * jnp.exp(e_col)).astype(BF16)
 
-    chain_copy = remote(
-        chain_out, chain_in, chain_send, chain_recv, ((sp + ny) % n_sp, tp)
-    )
+    loads[7].wait()
+    gate_out = dot(xn[...], wog_v[...])
+    og[...] = gate_out / (1.0 + jnp.exp(-gate_out))
 
     for k in range(1, ny):
         other = (y + k) % ny
@@ -299,38 +317,41 @@
             st.at[other], st.at[other], st_send.at[0], st_recv.at[other], (sp, partner)
         ).wait_recv()
 
-    def advance_chain():
+    def chain_copy(j):
+        return remote(
+            chain_out.at[j], chain_in.at[j], chain_send.at[j], chain_recv.at[j],
+            ((sp + ny) % n_sp, tp),
+        )
+
+    def advance_chain(received):
         for j in range(rec_heads):
-            rows_at = slice(j * STATE_ROWS, (j + 1) * STATE_ROWS)
-            state = chain_in[rows_at, :].astype(F32)
+            if received:
+                chain_copy(j).wait_recv()
+                state = chain_in[j].astype(F32)
+            else:
+                state = jnp.zeros((STATE_ROWS, STATE_ROWS), F32)
             for k in range(ny):
                 @pl.when(y == k)
                 def _():
-                    incoming[rows_at, :] = state.astype(BF16)
+                    incoming[j] = state.astype(BF16)
 
                 base = j * st_rows
                 decay = st[k, base + STATE_ROWS : base + st_rows, :].astype(F32)[0:1]
                 state = state * decay + st[k, base : base + STATE_ROWS, :].astype(F32)
-            chain_out[rows_at, :] = state.astype(BF16)
-
-        @pl.when(z < nz - 1)
-        def _():
-            chain_copy.start()
+            chain_out[j] = state.astype(BF16)
+
+            @pl.when(z < nz - 1)
+            def _():
+                chain_copy(j).start()
 
     @pl.when(z == 0)
     def _():
-        chain_in[...] = jnp.zeros_like(chain_in)
-        advance_chain()
+        advance_chain(False)
 
     def chain_at(here):
         @pl.when(here)
         def _():
-            chain_copy.wait_recv()
-            advance_chain()
-
-    loads[7].wait()
-    gate_out = dot(xn[...], wog_v[...])
-    og[...] = gate_out / (1.0 + jnp.exp(-gate_out))
+            advance_chain(True)
 
     for t in range(n_sp):
         @pl.when((sp != t) | jnp.logical_not(primary))
@@ -350,8 +371,8 @@
     for t in range(n_sp):
         ga[t] = jnp.where(lane_block == t, gate_parts, 0.0).astype(BF16)
 
-    def wait_all(ref, fwd, recv):
-        for t in range(n_sp):
+    def take(ref, fwd, recv, j):
+        for t in range(j * members, (j + 1) * members):
             copy = remote(ref.at[t], ref.at[t], fwd.at[t], recv.at[t], (sp, partner))
 
             @pl.when((sp != t) | jnp.logical_not(primary))
@@ -362,9 +383,11 @@
             def _():
                 copy.start()
 
-    chain_at(z == 1)
-    wait_all(k_all, k_fwd, k_recv)
-    chain_at(z == 2)
+    def take_keys(j):
+        take(k_all, k_fwd, k_recv, j)
+
+    def take_values(j):
+        take(v_all, v_fwd, v_recv, j)
 
     minus = jnp.where(
         iota((LANES, 2 * rows), 0) % 2 == iota((LANES, 2 * rows), 1) // rows, -1.0, 0.0
@@ -446,16 +469,23 @@
             o_in[src_head] = o_src[j]
             lg_in[src_head] = lg_src[j]
 
+    take_keys(0)
     for j in range(heads):
+        if j + 1 < heads:
+            take_keys(j + 1)
+        if j == heads - 1:
+            chain_at(z == 1)
+            take_values(0)
         weigh(j)
-    wait_all(v_all, v_fwd, v_recv)
     for j in range(heads):
+        if j + 1 < heads:
+            take_values(j + 1)
         finish(j)
-
-    chain_at(z >= 3)
+    chain_at(z >= 2)
+
     for j in range(rec_heads):
         lanes = slice(j * STATE_ROWS, (j + 1) * STATE_ROWS)
-        out = inner[:, lanes] + dot_nt(vq[:, lanes], incoming[lanes, :])
+        out = inner[:, lanes] + dot_nt(vq[:, lanes], incoming[j])
         mean = jnp.mean(out * out, axis=-1, keepdims=True)
         out = out * lax.rsqrt(mean + EPSILON) * r_gain[:, lanes] * og[:, lanes]
         vq[:, lanes] = out.astype(BF16)
@@ -541,7 +571,8 @@
 
     @pl.when(z < nz - 1)
     def _():
-        chain_copy.wait_send()
+        for j in range(rec_heads):
+            chain_copy(j).wait_send()
 
     for i in range(heads):
         for r in range(homes):
@@ -627,9 +658,7 @@
             pltpu.VMEM((rows, cols), F32),
             pltpu.VMEM((8, rows), F32),
             pltpu.VMEM((ny, rec_heads * (STATE_ROWS + 16), STATE_ROWS), BF16),
-            pltpu.VMEM((cols, STATE_ROWS), BF16),
-            pltpu.VMEM((cols, STATE_ROWS), BF16),
-            pltpu.VMEM((cols, STATE_ROWS), BF16),
+            *([pltpu.VMEM((rec_heads, STATE_ROWS, STATE_ROWS), BF16)] * 3),
             pltpu.VMEM((splits, rows, width // splits), BF16),
             *([pltpu.VMEM((chips, splits, rb, width // splits), BF16)] * 3),
             *([pltpu.VMEM((1, n), F32) for n in (width, HEAD_DIM, HEAD_DIM)]),
@@ -643,20 +672,20 @@
             dma((heads, homes)), dma((heads, homes)), dma((heads,)), dma((heads, homes, 2)),
             dma((n_sp,)), dma((n_sp,)), dma((heads,)), dma((n_sp,)), dma((n_sp,)), dma((n_sp,)),
             *([dma((heads,))] * 4),
-            dma((ny,)), dma((ny,)), dma, dma,
+            *([dma((ny,))] * 2), *([dma((rec_heads,))] * 2),
             *([dma((chips, splits))] * 4),
         ],
         compiler_params=pltpu.CompilerParams(
-            collective_id=0, has_side_effects=True, vmem_limit_bytes=60 * 1024 * 1024
+            collective_id=0, has_side_effects=True, vmem_limit_bytes=48 * 1024 * 1024
         ),
-    )(
+    )(*(pltpu.with_memory_space_constraint(a, pltpu.HBM) for a in (
         layer_input_rows, key_weight, value_weight, forget_weight, recurrence_value_weight,
         recurrence_query_weight, query_weight, output_gate_weight, attention_output_weight,
         recurrence_output_weight,
         input_norm_gain.reshape(1, -1), query_norm_gain.reshape(1, -1),
         key_norm_gain.reshape(1, -1), cumulative_gate.T, attention_norm_gain.reshape(1, -1),
         gate_lower_slack.reshape(1, -1), extra_log_decay.T, recurrence_norm_gain.reshape(1, -1),
-    )
+        )))
     return mixed, log_sum.T
 
 

time: 40.7 us -> 35 us (0.86)
  the two profiles are of different devices: /device:TPU:0 before, /device:TPU:25 now
where the time goes in v2:
time: 35 us; the launch traced here: 34.8 us
  Pallas kernels  32.9 us (94%)
  local copies, waits for them, and re-layouts  1.3 us (4%)
  between operations  0.65 us (2%)
    pallas_call x1, Pallas kernels, body(): pl.pallas_call(functools.partial(kernel, (nz, ny, n_tp)), name='mixer', o...  32.9 us
    unnamed x2, local copies, waits for them, and re-layouts  1.3 us

profile of v2, /device:TPU:25, one launch (start us, length us, event | category | flops | bytes accessed | tf_op | source)
XLA Modules:
  0.0 34.8 jit_solution(10233185128188090738)
XLA Ops:
  0.6 32.9 %mixer.1 = (bf16[64,2048]{1,0:T(8,128)(2,1)S(1)}, f32[4,256]{1,0:T(4,128)S(1)}) custom-call(bf16[256,2048]{1,0:T(8,128)(2,1)} %x_hbm.1, bf16[2048,256]{1,0:T(8,128)(2,1)} %wk_hbm.1, bf16[2048,256]{1,0:T(8,128)(2,1)} %wv_hbm.1, bf16[2048,256]{1,0:T(8,128)(2,1)} %wf_hbm.1, bf16[2048,256]{1,0:T(8,128)(2,1)} %wrv_hbm.1, bf16[2048,256]{1,0:T(8,128)(2,1)} %wrq_hbm.1, ...), custom_call_target="tpu_custom_call" | custom-call | tf_op jit(solution)/shard_map/mixer/pallas_call | solution.py:626
  33.5 0.7 %copy.22 = bf16[64,2048]{1,0:T(8,128)(2,1)} copy(bf16[64,2048]{1,0:T(8,128)(2,1)S(1)} %get-tuple-element.8) | data formatting | bytes 524288
  34.2 0.6 %copy.23 = f32[256,4]{0,1:T(4,128)} copy(f32[256,4]{0,1:T(4,128)S(1)} %bitcast.9) | data formatting | bytes 8192

commit v3 on v2

--- a/solution.py
+++ b/solution.py
@@ -52,12 +52,12 @@
     mixed_ref, logsum_ref,
     x_v, wkq_v, wfr_v, wvr_v, wog_v, wao_v, wro_v,
     xn, k_src, q_src, v_src, g_src, k_all, v_all, g_all, ga, q_in, s_buf, w_buf, m_s, l_s,
-    o_src, lg_src, o_in, lg_in,
-    inner, vq, og, ext, st, chain_in, chain_out, incoming, part, send2, recv1, recv2,
+    o_src, lg_src, o_in, lg_in, attn_out,
+    inner, vq, og, ext, st, up_in, up_out, chain_in, chain_out, incoming, part, send2, recv1, recv2,
     in_gain, q_gain, k_gain, gate_t, a_gain, slack, extra_t, r_gain, rec_part,
     load_sem, k_send, v_send, q_send, g_send, k_recv, v_recv, q_recv, g_recv, k_fwd, v_fwd,
     o_send, o_recv, lg_send, lg_recv,
-    st_send, st_recv, chain_send, chain_recv,
+    st_send, st_recv, up_send, up_recv, chain_send, chain_recv,
     s1_send, s1_recv, s2_send, s2_recv,
 ):
     nz, ny, ntp = sizes
@@ -70,7 +70,7 @@
     chips = ntp // 2
     rb = rows // ntp
     half = rows // 2
-    splits = s1_send.shape[1]
+    splits = s1_recv.shape[1]
     part_cols = width // splits
     homes = n_sp // (2 * heads)
     members = 2 * homes
@@ -107,10 +107,13 @@
         (gate_t_hbm, gate_t), (a_gain_hbm, a_gain), (slack_hbm, slack),
         (extra_t_hbm, extra_t), (r_gain_hbm, r_gain),
     )):
-        loads.append(pltpu.make_async_copy(src, dst, load_sem.at[i]))
+        loads.append(pltpu.make_async_copy(src, dst, load_sem.at[i - 1 if i in (2, 4, 6) else i]))
 
     for copy in loads[:1] + loads[10:] + loads[1:3]:
         copy.start()
+
+    def both(ref, i):
+        pltpu.make_async_copy(ref, ref, load_sem.at[i]).wait()
 
     barrier = pltpu.get_barrier_semaphore()
 
@@ -145,8 +148,7 @@
         gain = jnp.concatenate([gain_ref[...]] * heads, axis=1)
         return v * lax.rsqrt(mean + EPSILON) * gain
 
-    loads[1].wait()
-    loads[2].wait()
+    both(wkq_v, 1)
     for copy in loads[5:7]:
         copy.start()
     kq = dot(xn[...], wkq_v[...])
@@ -169,25 +171,41 @@
 
     def k_copy(i, r):
         return remote(
-            k_src.at[i], k_all.at[sp], k_send.at[i, r], k_recv.at[sp], (home_of(i, r), tp)
+            k_src.at[i], k_all.at[sp], k_send, k_recv.at[my_j], (home_of(i, r), tp)
         )
 
     def v_copy(i, r):
         return remote(
-            v_src.at[i], v_all.at[sp], v_send.at[i, r], v_recv.at[sp], (home_of(i, r), tp)
+            v_src.at[i], v_all.at[sp], v_send, v_recv.at[my_j], (home_of(i, r), tp)
         )
 
     def g_copy(i, r, c):
         return remote(
-            g_src.at[i], g_all.at[sp], g_send.at[i, r, c], g_recv.at[sp],
-            (home_of(i, r), tp if c == 0 else partner),
+            g_src.at[i], g_all.at[sp], g_send, g_recv, (home_of(i, r), tp if c == 0 else partner)
         )
 
     def q_copy(i):
         return remote(
-            q_src.at[i], q_in.at[my_j], q_send.at[i], q_recv.at[my_j],
+            q_src.at[i], q_in.at[my_j], q_send, q_recv.at[my_j],
             (home_of(i, my_home), chip * 2 + my_core),
         )
+
+    def sent(ref, sem):
+        remote(ref, ref, sem, g_recv, (sp, partner)).wait_send()
+
+    def landed(ref, sem):
+        remote(ref, ref, g_send, sem, (sp, partner)).wait_recv()
+
+    def either(here, act, ref, few, many):
+        @pl.when(here)
+        def _():
+            act(ref.at[0:few])
+
+        @pl.when(jnp.logical_not(here))
+        def _():
+            act(ref.at[0:many])
+
+    own = primary & (member == my_member)
 
     turns = [(src_head + k) % heads for k in range(heads)]
 
@@ -221,7 +239,7 @@
                 g_copy(i, r, 1).start()
         spread(k_copy, keep_k)
         for i in turns:
-            stays = (home_of(i, my_home) == sp) & (my_core == core)
+            stays = own & (i == src_head)
 
             @pl.when(jnp.logical_not(stays))
             def _():
@@ -240,8 +258,7 @@
 
     tri = iota((rows, rows), 0) >= iota((rows, rows), 1)
     tri_b = tri.astype(F32).astype(BF16)
-    loads[3].wait()
-    loads[4].wait()
+    both(wfr_v, 3)
     for copy in loads[7:10]:
         copy.start()
     fr = dot(xn[...], wfr_v[...])
@@ -269,8 +286,10 @@
 
     def st_copy(k):
         return remote(
-            st.at[y], st.at[y], st_send.at[k], st_recv.at[y], (z * ny + (y + k) % ny, tp)
-        )
+            st.at[y], st.at[y], st_send, st_recv, (z * ny + (y + k) % ny, tp)
+        )
+
+    lifts = (z % 2 == 0) & (z + 1 < nz)
 
     @pl.when(early)
     def _():
@@ -283,8 +302,7 @@
     def _():
         send_keys_and_queries()
 
-    loads[5].wait()
-    loads[6].wait()
+    both(wvr_v, 5)
     vr = dot(xn[...], wvr_v[...])
     values_t = vr[:, 0:cols].T.astype(BF16)
     for i in range(heads):
@@ -311,54 +329,77 @@
     gate_out = dot(xn[...], wog_v[...])
     og[...] = gate_out / (1.0 + jnp.exp(-gate_out))
 
-    for k in range(1, ny):
-        other = (y + k) % ny
-        remote(
-            st.at[other], st.at[other], st_send.at[0], st_recv.at[other], (sp, partner)
-        ).wait_recv()
-
-    def chain_copy(j):
-        return remote(
-            chain_out.at[j], chain_in.at[j], chain_send.at[j], chain_recv.at[j],
-            ((sp + ny) % n_sp, tp),
-        )
-
-    def advance_chain(received):
+    def up_copy(j):
+        return remote(
+            up_out.at[j], up_in.at[j], up_send, up_recv.at[j], ((sp + ny) % n_sp, tp)
+        )
+
+    def chain_copy(j, d):
+        return remote(
+            chain_out.at[j], chain_in.at[j], chain_send.at[d - 1], chain_recv.at[j],
+            ((sp + d * ny) % n_sp, tp),
+        )
+
+    def added(j, k):
+        base = j * st_rows
+        return (
+            st[k, base : base + STATE_ROWS, :].astype(F32),
+            st[k, base + STATE_ROWS : base + st_rows, :].astype(F32),
+        )
+
+    def states_of_row():
+        if ny > 1:
+            landed(st.at[0 : ny - 1], st_recv)
+
+    def lift():
         for j in range(rec_heads):
+            total, kept = added(j, 0)
+            for k in range(1, ny):
+                more, decay = added(j, k)
+                total, kept = total * decay[0:1] + more, kept * decay
+            up_out[j, 0:STATE_ROWS, :] = total.astype(BF16)
+            up_out[j, STATE_ROWS:st_rows, :] = kept.astype(BF16)
+            up_copy(j).start()
+
+    def advance(received, odd):
+        for j in range(rec_heads):
+            state = jnp.zeros((STATE_ROWS, STATE_ROWS), F32)
             if received:
-                chain_copy(j).wait_recv()
+                landed(chain_in.at[j], chain_recv.at[j])
                 state = chain_in[j].astype(F32)
-            else:
-                state = jnp.zeros((STATE_ROWS, STATE_ROWS), F32)
+            if odd:
+                landed(up_in.at[j], up_recv.at[j])
+                decay = up_in[j, STATE_ROWS:st_rows, :].astype(F32)[0:1]
+                state = state * decay + up_in[j, 0:STATE_ROWS, :].astype(F32)
             for k in range(ny):
                 @pl.when(y == k)
                 def _():
                     incoming[j] = state.astype(BF16)
 
-                base = j * st_rows
-                decay = st[k, base + STATE_ROWS : base + st_rows, :].astype(F32)[0:1]
-                state = state * decay + st[k, base : base + STATE_ROWS, :].astype(F32)
-            chain_out[j] = state.astype(BF16)
-
-            @pl.when(z < nz - 1)
-            def _():
-                chain_copy(j).start()
-
-    @pl.when(z == 0)
+                if odd or k + 1 < ny:
+                    more, decay = added(j, k)
+                    state = state * decay[0:1] + more
+            if odd:
+                chain_out[j] = state.astype(BF16)
+                for d in (1, 2):
+                    @pl.when(z + d < nz)
+                    def _():
+                        chain_copy(j, d).start()
+
+    def advance_at(where, received, odd):
+        @pl.when(where & (z % 2 == odd))
+        def _():
+            advance(received, odd)
+
+    states_of_row()
+
+    @pl.when(lifts)
     def _():
-        advance_chain(False)
-
-    def chain_at(here):
-        @pl.when(here)
-        def _():
-            advance_chain(True)
-
-    for t in range(n_sp):
-        @pl.when((sp != t) | jnp.logical_not(primary))
-        def _():
-            remote(
-                g_all.at[t], g_all.at[t], g_send.at[0, 0, 0], g_recv.at[t], (sp, partner)
-            ).wait_recv()
+        lift()
+
+    advance_at(z < 2, False, 0)
+
+    either(primary, lambda ref: landed(ref, g_recv), g_all, n_sp - 1, n_sp)
 
     gate_cols = jnp.concatenate(
         [g_all[t, :, h * half : (h + 1) * half] for t in range(n_sp) for h in range(2)], axis=0
@@ -372,16 +413,15 @@
         ga[t] = jnp.where(lane_block == t, gate_parts, 0.0).astype(BF16)
 
     def take(ref, fwd, recv, j):
-        for t in range(j * members, (j + 1) * members):
-            copy = remote(ref.at[t], ref.at[t], fwd.at[t], recv.at[t], (sp, partner))
-
-            @pl.when((sp != t) | jnp.logical_not(primary))
-            def _():
-                copy.wait_recv()
-
-            @pl.when(primary)
-            def _():
-                copy.start()
+        either(
+            primary & (my_j == j), lambda part: landed(part, recv.at[j]), ref,
+            members - 1, members,
+        )
+
+        @pl.when(primary)
+        def _():
+            for t in range(j * members, (j + 1) * members):
+                remote(ref.at[t], ref.at[t], fwd, recv.at[j], (sp, partner)).start()
 
     def take_keys(j):
         take(k_all, k_fwd, k_recv, j)
@@ -399,16 +439,9 @@
     first = [members * j * (j + 1) // 2 for j in range(heads)]
 
     def weigh(j):
-        remote(
-            q_in.at[j], q_in.at[j], q_send.at[0], q_recv.at[j], (sp, partner)
-        )
-        kept = (block_of(j) == sp) & primary
-
-        @pl.when(jnp.logical_not(kept))
+        @pl.when(jnp.logical_not(own & (my_j == j)))
         def _():
-            remote(
-                q_in.at[j], q_in.at[j], q_send.at[0], q_recv.at[j], (sp, partner)
-            ).wait_recv()
+            landed(q_in.at[j], q_recv.at[j])
 
         q = q_in[j]
         none = jnp.zeros_like(q)
@@ -438,14 +471,12 @@
 
     def o_copy(j):
         return remote(
-            o_src.at[j], o_in.at[src_head], o_send.at[j], o_recv.at[src_head],
-            (block_of(j), src_tp),
+            o_src.at[j], o_in.at[src_head], o_send, o_recv, (block_of(j), src_tp)
         )
 
     def lg_copy(j):
         return remote(
-            lg_src.at[j], lg_in.at[src_head], lg_send.at[j], lg_recv.at[src_head],
-            (block_of(j), src_tp),
+            lg_src.at[j], lg_in.at[src_head], lg_send, lg_recv, (block_of(j), src_tp)
         )
 
     def finish(j):
@@ -457,7 +488,7 @@
         mean = jnp.mean(out * out, axis=0, keepdims=True)
         o_src[j] = (out * lax.rsqrt(mean + EPSILON)).astype(BF16)
         lg_src[j] = m_s[j] + jnp.log(l_s[j])
-        kept = (block_of(j) == sp) & primary
+        kept = own & (my_j == j)
 
         @pl.when(jnp.logical_not(kept))
         def _():
@@ -469,19 +500,24 @@
             o_in[src_head] = o_src[j]
             lg_in[src_head] = lg_src[j]
 
+    def finish_next(j):
+        take_values(j)
+        finish(j)
+
+    lag = 2
     take_keys(0)
     for j in range(heads):
         if j + 1 < heads:
             take_keys(j + 1)
-        if j == heads - 1:
-            chain_at(z == 1)
-            take_values(0)
         weigh(j)
-    for j in range(heads):
-        if j + 1 < heads:
-            take_values(j + 1)
-        finish(j)
-    chain_at(z >= 2)
+        if j + 1 == max(heads - 1, 1):
+            advance_at(z < 2, False, 1)
+        if j >= lag:
+            finish_next(j - lag)
+    for j in range(max(heads - lag, 0), heads):
+        finish_next(j)
+    advance_at(z >= 2, True, 0)
+    advance_at(z >= 2, True, 1)
 
     for j in range(rec_heads):
         lanes = slice(j * STATE_ROWS, (j + 1) * STATE_ROWS)
@@ -493,22 +529,13 @@
     rec_part[...] = dot(vq[...], wro_v[...])
     loads[8].wait()
 
-    for i in range(heads):
-        kept = (home_of(i, my_home) == sp) & (my_core == core)
-
-        @pl.when(jnp.logical_not(kept))
-        def _():
-            remote(
-                o_in.at[i], o_in.at[i], o_send.at[0], o_recv.at[i], (sp, partner)
-            ).wait_recv()
-            remote(
-                lg_in.at[i], lg_in.at[i], lg_send.at[0], lg_recv.at[i], (sp, partner)
-            ).wait_recv()
+    either(own, lambda ref: landed(ref, o_recv), o_in, heads - 1, heads)
+    either(own, lambda ref: landed(ref, lg_recv), lg_in, heads - 1, heads)
 
     for i in range(heads):
         logsum_ref[i : i + 1, :] = lg_in[i] + gate_t[i : i + 1, :]
     attn_t = jnp.concatenate([o_in[i].astype(F32) for i in range(heads)], axis=0)
-    attn_out = (attn_t.T * a_gain[...]).astype(BF16)
+    attn_out[...] = (attn_t.T * a_gain[...]).astype(BF16)
 
     def rows_of(which_chip, which_core):
         return pl.ds(pl.multiple_of((which_chip * 2 + which_core) * rb, rb), rb)
@@ -519,13 +546,13 @@
     def within(j, q):
         return pltpu.make_async_remote_copy(
             src_ref=part.at[q, rows_of(j, 1 - core)], dst_ref=recv1.at[j, q],
-            send_sem=s1_send.at[j, q], recv_sem=s1_recv.at[j, q], device_id=(sp, partner),
+            send_sem=s1_send, recv_sem=s1_recv.at[j, q], device_id=(sp, partner),
             device_id_type=MESH,
         )
 
     def between(j, q):
         return pltpu.make_async_remote_copy(
-            src_ref=send2.at[j, q], dst_ref=recv2.at[chip, q], send_sem=s2_send.at[j, q],
+            src_ref=send2.at[j, q], dst_ref=recv2.at[chip, q], send_sem=s2_send,
             recv_sem=s2_recv.at[chip, q], device_id=(sp, j * 2 + core), device_id_type=MESH,
         )
 
@@ -540,65 +567,69 @@
             send2[j, q] = chip_sum(j, q).astype(BF16)
             between(j, q).start()
 
+    def partial_of(j, q):
+        at = pl.ds(pl.multiple_of(j * 2 * rb, 2 * rb), 2 * rb)
+        part[q, at, :] = (
+            dot(attn_out[at, :], wao_v[:, columns(q)]) + rec_part[at, columns(q)]
+        ).astype(BF16)
+        within(j, q).start()
+
     for q in range(splits):
-        part[q] = (
-            dot(attn_out, wao_v[:, columns(q)]) + rec_part[:, columns(q)]
-        ).astype(BF16)
         for j in order:
-            within(j, q).start()
+            partial_of(j, q)
         if q > 0:
             send_sums(q - 1)
     send_sums(splits - 1)
     for q in range(splits):
-        within(chip, q).start()
+        partial_of(chip, q)
     for q in range(splits):
         total = chip_sum(chip, q)
         for j in order:
             pltpu.make_async_remote_copy(
-                src_ref=send2.at[j, q], dst_ref=recv2.at[j, q], send_sem=s2_send.at[j, q],
+                src_ref=send2.at[j, q], dst_ref=recv2.at[j, q], send_sem=s2_send,
                 recv_sem=s2_recv.at[j, q], device_id=(sp, partner), device_id_type=MESH,
             ).wait_recv()
             total = total + recv2[j, q].astype(F32)
         mixed_ref[:, columns(q)] = total.astype(BF16)
 
-    for q in range(splits):
-        for j in order + [chip]:
-            within(j, q).wait_send()
-        for j in order:
-            between(j, q).wait_send()
-    for k in range(1, ny):
-        st_copy(k).wait_send()
-
-    @pl.when(z < nz - 1)
+    sent(recv1, s1_send)
+    if chips > 1:
+        sent(recv2.at[0 : chips - 1], s2_send)
+    if ny > 1:
+        sent(st.at[0 : ny - 1], st_send)
+
+    @pl.when(lifts)
     def _():
-        for j in range(rec_heads):
-            chain_copy(j).wait_send()
-
-    for i in range(heads):
-        for r in range(homes):
-            @pl.when(home_of(i, r) != sp)
-            def _():
-                k_copy(i, r).wait_send()
-                v_copy(i, r).wait_send()
-                g_copy(i, r, 0).wait_send()
-
-            g_copy(i, r, 1).wait_send()
-
-        @pl.when((home_of(i, my_home) != sp) | (my_core != core))
+        sent(up_out, up_send)
+
+    for d in (1, 2):
+        @pl.when((z % 2 == 1) & (z + d < nz))
         def _():
-            q_copy(i).wait_send()
+            sent(chain_out, chain_send.at[d - 1])
+
+    copies = heads * homes
+    either(primary, lambda ref: sent(ref, k_send), k_all, copies - 1, copies)
+    either(primary, lambda ref: sent(ref, v_send), v_all, copies - 1, copies)
+    either(primary, lambda ref: sent(ref, g_send), g_all, n_sp - 1, n_sp)
+    either(own, lambda ref: sent(ref, q_send), q_in, heads - 1, heads)
+    either(own, lambda ref: sent(ref, o_send), o_in, heads - 1, heads)
+    either(own, lambda ref: sent(ref, lg_send), lg_in, heads - 1, heads)
 
     @pl.when(primary)
     def _():
-        for t in range(n_sp):
-            remote(k_all.at[t], k_all.at[t], k_fwd.at[t], k_recv.at[t], (sp, partner)).wait_send()
-            remote(v_all.at[t], v_all.at[t], v_fwd.at[t], v_recv.at[t], (sp, partner)).wait_send()
-
-    for j in range(heads):
-        @pl.when((block_of(j) != sp) | jnp.logical_not(primary))
-        def _():
-            o_copy(j).wait_send()
-            lg_copy(j).wait_send()
+        sent(k_all, k_fwd)
+        sent(v_all, v_fwd)
+
+
+def leave(mixed_v, log_sum_v, mixed_hbm, log_sum_hbm, sem):
+    copies = (
+        pltpu.make_async_copy(mixed_v, mixed_hbm, sem.at[0]),
+        pltpu.make_async_copy(log_sum_v, log_sum_hbm, sem.at[1]),
+    )
+    for copy in copies:
+        copy.start()
+    for copy in copies:
+        copy.wait()
 
 
 def body(
@@ -653,11 +684,13 @@
             pltpu.VMEM((heads, 1, rows), F32),
             pltpu.VMEM((heads, HEAD_DIM, rows), BF16),
             pltpu.VMEM((heads, 1, rows), F32),
+            pltpu.VMEM((rows, cols), BF16),
             pltpu.VMEM((rows, cols), F32),
             pltpu.VMEM((rows, cols), BF16),
             pltpu.VMEM((rows, cols), F32),
             pltpu.VMEM((8, rows), F32),
             pltpu.VMEM((ny, rec_heads * (STATE_ROWS + 16), STATE_ROWS), BF16),
+            *([pltpu.VMEM((rec_heads, STATE_ROWS + 16, STATE_ROWS), BF16)] * 2),
             *([pltpu.VMEM((rec_heads, STATE_ROWS, STATE_ROWS), BF16)] * 3),
             pltpu.VMEM((splits, rows, width // splits), BF16),
             *([pltpu.VMEM((chips, splits, rb, width // splits), BF16)] * 3),
@@ -669,11 +702,11 @@
             pltpu.VMEM((1, cols), F32),
             pltpu.VMEM((rows, width), F32),
             dma((18,)),
-            dma((heads, homes)), dma((heads, homes)), dma((heads,)), dma((heads, homes, 2)),
-            dma((n_sp,)), dma((n_sp,)), dma((heads,)), dma((n_sp,)), dma((n_sp,)), dma((n_sp,)),
-            *([dma((heads,))] * 4),
-            *([dma((ny,))] * 2), *([dma((rec_heads,))] * 2),
-            *([dma((chips, splits))] * 4),
+            dma, dma, dma, dma,
+            *([dma((heads,))] * 3), dma, dma, dma,
+            dma, dma, dma, dma,
+            dma, dma, dma, dma((rec_heads,)), dma((2,)), dma((rec_heads,)),
+            dma, dma((chips, splits)), dma, dma((chips, splits)),
         ],
         compiler_params=pltpu.CompilerParams(
             collective_id=0, has_side_effects=True, vmem_limit_bytes=48 * 1024 * 1024
@@ -686,6 +719,18 @@
         key_norm_gain.reshape(1, -1), cumulative_gate.T, attention_norm_gain.reshape(1, -1),
         gate_lower_slack.reshape(1, -1), extra_log_decay.T, recurrence_norm_gain.reshape(1, -1),
         )))
+    mixed, log_sum = pl.pallas_call(
+        leave,
+        name="leave",
+        out_shape=(
+            jax.ShapeDtypeStruct((rb, width), BF16),
+            jax.ShapeDtypeStruct((heads, rows), F32),
+        ),
+        in_specs=[vmem] * 2,
+        out_specs=(any_space, any_space),
+        scratch_shapes=[dma((2,))],
+        compiler_params=pltpu.CompilerParams(vmem_limit_bytes=4 * 1024 * 1024),
+    )(mixed, log_sum)
     return mixed, log_sum.T
 
 

time: 35 us -> 32.9 us (0.940)
  local copies, waits for them, and re-layouts: 1.3 us -> 0 us
  Pallas kernels: 32.9 us -> 32.1 us
    pallas_call x1, Pallas kernels: 32.9 us -> 31.3 us  [body(): pl.pallas_call(functools.partial(kernel, (nz, ny, n_tp)), name='mixer', o...]
    unnamed x2 -> x0, local copies, waits for them, and re-layouts: 1.3 us -> none
    pallas_call x0 -> x1, Pallas kernels: none -> 0.72 us  [body(): pl.pallas_call(leave, name='leave', out_shape=(jax.ShapeDtypeStruct((rb,...]
where the time goes in v3:
time: 32.9 us; the launch traced here: 32.7 us
  Pallas kernels  32.1 us (98%)
  between operations  0.65 us (2%)
    pallas_call x1, Pallas kernels, body(): pl.pallas_call(functools.partial(kernel, (nz, ny, n_tp)), name='mixer', o...  31.3 us
    pallas_call x1, Pallas kernels, body(): pl.pallas_call(leave, name='leave', out_shape=(jax.ShapeDtypeStruct((rb,...  0.72 us

profile of v3, /device:TPU:25, one launch (start us, length us, event | category | flops | bytes accessed | tf_op | source)
XLA Modules:
  0.0 32.7 jit_solution(16176427974740470327)
XLA Ops:
  0.6 31.3 %mixer.1 = (bf16[64,2048]{1,0:T(8,128)(2,1)S(1)}, f32[4,256]{1,0:T(4,128)S(1)}) custom-call(bf16[256,2048]{1,0:T(8,128)(2,1)} %x_hbm.1, bf16[2048,256]{1,0:T(8,128)(2,1)} %wk_hbm.1, bf16[2048,256]{1,0:T(8,128)(2,1)} %wv_hbm.1, bf16[2048,256]{1,0:T(8,128)(2,1)} %wf_hbm.1, bf16[2048,256]{1,0:T(8,128)(2,1)} %wrv_hbm.1, bf16[2048,256]{1,0:T(8,128)(2,1)} %wrq_hbm.1, ...), custom_call_target="tpu_custom_call" | custom-call | tf_op jit(solution)/shard_map/mixer/pallas_call | solution.py:657
  32.0 0.7 %leave.1 = (bf16[64,2048]{1,0:T(8,128)(2,1)}, f32[4,256]{1,0:T(4,128)}) custom-call(bf16[64,2048]{1,0:T(8,128)(2,1)S(1)} %get-tuple-element.6.mixed_v, f32[4,256]{1,0:T(4,128)S(1)} %get-tuple-element.7.log_sum_v), custom_call_target="tpu_custom_call" | custom-call | tf_op jit(solution)/shard_map/leave/pallas_call | solution.py:722

commit v4 on v3

--- a/solution.py
+++ b/solution.py
@@ -50,11 +50,11 @@
     in_gain_hbm, q_gain_hbm, k_gain_hbm, gate_t_hbm, a_gain_hbm,
     slack_hbm, extra_t_hbm, r_gain_hbm,
     mixed_ref, logsum_ref,
-    x_v, wkq_v, wfr_v, wvr_v, wog_v, wao_v, wro_v,
+    x_v, wkq_v, wfr_v, wvr_v, wog_v, wo_v,
     xn, k_src, q_src, v_src, g_src, k_all, v_all, g_all, ga, q_in, s_buf, w_buf, m_s, l_s,
-    o_src, lg_src, o_in, lg_in, attn_out,
+    o_src, lg_src, o_in, lg_in, mix,
     inner, vq, og, ext, st, up_in, up_out, chain_in, chain_out, incoming, part, send2, recv1, recv2,
-    in_gain, q_gain, k_gain, gate_t, a_gain, slack, extra_t, r_gain, rec_part,
+    in_gain, q_gain, k_gain, gate_t, a_gain, slack, extra_t, r_gain,
     load_sem, k_send, v_send, q_send, g_send, k_recv, v_recv, q_recv, g_recv, k_fwd, v_fwd,
     o_send, o_recv, lg_send, lg_recv,
     st_send, st_recv, up_send, up_recv, chain_send, chain_recv,
@@ -102,12 +102,13 @@
         (x_hbm, x_v), (wk_hbm, wkq_v.at[:, 0:cols]), (wq_hbm, wkq_v.at[:, cols : 2 * cols]),
         (wf_hbm, wfr_v.at[:, 0:cols]), (wrv_hbm, wfr_v.at[:, cols : 2 * cols]),
         (wv_hbm, wvr_v.at[:, 0:cols]), (wrq_hbm, wvr_v.at[:, cols : 2 * cols]),
-        (wog_hbm, wog_v), (wao_hbm, wao_v), (wro_hbm, wro_v),
+        (wog_hbm, wog_v), (wao_hbm, wo_v.at[0:cols, :]),
+        (wro_hbm, wo_v.at[cols : 2 * cols, :]),
         (in_gain_hbm, in_gain), (q_gain_hbm, q_gain), (k_gain_hbm, k_gain),
         (gate_t_hbm, gate_t), (a_gain_hbm, a_gain), (slack_hbm, slack),
         (extra_t_hbm, extra_t), (r_gain_hbm, r_gain),
     )):
-        loads.append(pltpu.make_async_copy(src, dst, load_sem.at[i - 1 if i in (2, 4, 6) else i]))
+        loads.append(pltpu.make_async_copy(src, dst, load_sem.at[i - 1 if i in (4, 6) else i]))
 
     for copy in loads[:1] + loads[10:] + loads[1:3]:
         copy.start()
@@ -148,21 +149,18 @@
         gain = jnp.concatenate([gain_ref[...]] * heads, axis=1)
         return v * lax.rsqrt(mean + EPSILON) * gain
 
-    both(wkq_v, 1)
-    for copy in loads[5:7]:
-        copy.start()
-    kq = dot(xn[...], wkq_v[...])
-    keys = head_norm(kq[:, 0:cols], k_gain)
+    def by_halves(lanes):
+        w = wkq_v[:, lanes]
+        return jnp.concatenate([dot(xn[0:half, :], w), dot(xn[half:rows, :], w)], axis=0)
+
+    loads[1].wait()
+    keys = head_norm(by_halves(slice(0, cols)), k_gain)
     first_half = iota((half, LANES), 1) < HEAD_DIM
     for p in range(pairs):
         low = keys[0:half, p * LANES : (p + 1) * LANES]
         high = keys[half:rows, p * LANES : (p + 1) * LANES]
         k_src[2 * p] = jnp.where(first_half, low, pltpu.roll(high, HEAD_DIM, 1)).astype(BF16)
         k_src[2 * p + 1] = jnp.where(first_half, pltpu.roll(low, HEAD_DIM, 1), high).astype(BF16)
-    queries_t = (head_norm(kq[:, cols : 2 * cols], q_gain).astype(BF16).astype(F32)).T
-    for i in range(heads):
-        q_src[i] = (queries_t[i * HEAD_DIM : (i + 1) * HEAD_DIM, :] * HEAD_DIM ** (-0.5)).astype(BF16)
-
     def remote(src, dst, send, recv, where):
         return pltpu.make_async_remote_copy(
             src_ref=src, dst_ref=dst, send_sem=send, recv_sem=recv,
@@ -232,12 +230,14 @@
     def begin():
         pl.semaphore_wait(barrier, 2 * n_sp - 1 + chips - 1)
 
-    def send_keys_and_queries():
+    def send_keys():
         spread(lambda i, r: g_copy(i, r, 0), keep_g)
         for i in range(heads):
             for r in range(homes):
                 g_copy(i, r, 1).start()
         spread(k_copy, keep_k)
+
+    def send_queries():
         for i in turns:
             stays = own & (i == src_head)
 
@@ -254,7 +254,19 @@
     @pl.when(jnp.logical_not(early))
     def _():
         begin()
-        send_keys_and_queries()
+        send_keys()
+
+    loads[2].wait()
+    for copy in loads[5:7]:
+        copy.start()
+    queries = head_norm(by_halves(slice(cols, 2 * cols)), q_gain)
+    queries_t = (queries.astype(BF16).astype(F32) * HEAD_DIM ** (-0.5)).T.astype(BF16)
+    for i in range(heads):
+        q_src[i] = queries_t[i * HEAD_DIM : (i + 1) * HEAD_DIM, :]
+
+    @pl.when(jnp.logical_not(early))
+    def _():
+        send_queries()
 
     tri = iota((rows, rows), 0) >= iota((rows, rows), 1)
     tri_b = tri.astype(F32).astype(BF16)
@@ -300,7 +312,8 @@
 
     @pl.when(early)
     def _():
-        send_keys_and_queries()
+        send_keys()
+        send_queries()
 
     both(wvr_v, 5)
     vr = dot(xn[...], wvr_v[...])
@@ -438,11 +451,12 @@
     )
     first = [members * j * (j + 1) // 2 for j in range(heads)]
 
-    def weigh(j):
+    def take_query(j):
         @pl.when(jnp.logical_not(own & (my_j == j)))
         def _():
             landed(q_in.at[j], q_recv.at[j])
 
+    def weigh(j):
         q = q_in[j]
         none = jnp.zeros_like(q)
         right = jnp.concatenate(
@@ -488,6 +502,8 @@
         mean = jnp.mean(out * out, axis=0, keepdims=True)
         o_src[j] = (out * lax.rsqrt(mean + EPSILON)).astype(BF16)
         lg_src[j] = m_s[j] + jnp.log(l_s[j])
+
+    def give(j):
         kept = own & (my_j == j)
 
         @pl.when(jnp.logical_not(kept))
@@ -500,22 +516,19 @@
             o_in[src_head] = o_src[j]
             lg_in[src_head] = lg_src[j]
 
-    def finish_next(j):
-        take_values(j)
-        finish(j)
-
-    lag = 2
-    take_keys(0)
-    for j in range(heads):
-        if j + 1 < heads:
-            take_keys(j + 1)
-        weigh(j)
-        if j + 1 == max(heads - 1, 1):
-            advance_at(z < 2, False, 1)
-        if j >= lag:
-            finish_next(j - lag)
-    for j in range(max(heads - lag, 0), heads):
-        finish_next(j)
+    def each(jobs, *acts):
+        for act in acts:
+            for j in jobs:
+                act(j)
+
+    at = max(heads - 2, 1)
+    each(range(at), take_keys, take_query, weigh)
+    each(range(at, heads), take_keys, take_query)
+    advance_at(z < 2, False, 1)
+    each((0,), take_values, finish, give)
+    each(range(at, heads), weigh)
+    each(range(1, heads - 1), take_values, finish, give)
+    each((heads - 1,), take_values, finish, give)
     advance_at(z >= 2, True, 0)
     advance_at(z >= 2, True, 1)
 
@@ -524,9 +537,8 @@
         out = inner[:, lanes] + dot_nt(vq[:, lanes], incoming[j])
         mean = jnp.mean(out * out, axis=-1, keepdims=True)
         out = out * lax.rsqrt(mean + EPSILON) * r_gain[:, lanes] * og[:, lanes]
-        vq[:, lanes] = out.astype(BF16)
+        mix[:, cols + j * STATE_ROWS : cols + (j + 1) * STATE_ROWS] = out.astype(BF16)
     loads[9].wait()
-    rec_part[...] = dot(vq[...], wro_v[...])
     loads[8].wait()
 
     either(own, lambda ref: landed(ref, o_recv), o_in, heads - 1, heads)
@@ -535,7 +547,7 @@
     for i in range(heads):
         logsum_ref[i : i + 1, :] = lg_in[i] + gate_t[i : i + 1, :]
     attn_t = jnp.concatenate([o_in[i].astype(F32) for i in range(heads)], axis=0)
-    attn_out[...] = (attn_t.T * a_gain[...]).astype(BF16)
+    mix[:, 0:cols] = (attn_t.T * a_gain[...]).astype(BF16)
 
     def rows_of(which_chip, which_core):
         return pl.ds(pl.multiple_of((which_chip * 2 + which_core) * rb, rb), rb)
@@ -569,9 +581,7 @@
 
     def partial_of(j, q):
         at = pl.ds(pl.multiple_of(j * 2 * rb, 2 * rb), 2 * rb)
-        part[q, at, :] = (
-            dot(attn_out[at, :], wao_v[:, columns(q)]) + rec_part[at, columns(q)]
-        ).astype(BF16)
+        part[q, at, :] = dot(mix[at, :], wo_v[:, columns(q)]).astype(BF16)
         within(j, q).start()
 
     for q in range(splits):
@@ -650,7 +660,6 @@
     splits = math.gcd(width // LANES, 4)
     weight = pltpu.VMEM((width, cols), BF16)
     two_weights = pltpu.VMEM((width, 2 * cols), BF16)
-    out_weight = pltpu.VMEM((cols, width), BF16)
     dma = pltpu.SemaphoreType.DMA
     any_space = pl.BlockSpec(memory_space=pl.ANY)
     vmem = pl.BlockSpec(memory_space=pltpu.VMEM)
@@ -665,7 +674,7 @@
         out_specs=(vmem, vmem),
         scratch_shapes=[
             pltpu.VMEM((rows, width), BF16),
-            *([two_weights] * 3), weight, out_weight, out_weight,
+            *([two_weights] * 3), weight, pltpu.VMEM((2 * cols, width), BF16),
             pltpu.VMEM((rows, width), BF16),
             pltpu.VMEM((heads, half, LANES), BF16),
             pltpu.VMEM((heads, HEAD_DIM, rows), BF16),
@@ -684,7 +693,7 @@
             pltpu.VMEM((heads, 1, rows), F32),
             pltpu.VMEM((heads, HEAD_DIM, rows), BF16),
             pltpu.VMEM((heads, 1, rows), F32),
-            pltpu.VMEM((rows, cols), BF16),
+            pltpu.VMEM((rows, 2 * cols), BF16),
             pltpu.VMEM((rows, cols), F32),
             pltpu.VMEM((rows, cols), BF16),
             pltpu.VMEM((rows, cols), F32),
@@ -700,7 +709,6 @@
             pltpu.VMEM((1, cols), F32),
             pltpu.VMEM((rec_heads, rows), F32),
             pltpu.VMEM((1, cols), F32),
-            pltpu.VMEM((rows, width), F32),
             dma((18,)),
             dma, dma, dma, dma,
             *([dma((heads,))] * 3), dma, dma, dma,

time: 32.9 us -> 32.3 us (0.982); the launches traced: 32.7 us -> 31.8 us
  Pallas kernels: 32.1 us -> 31.1 us
    pallas_call x1, Pallas kernels: 31.3 us -> 30.4 us  [body(): pl.pallas_call(functools.partial(kernel, (nz, ny, n_tp)), name='mixer', o...]
where the time goes in v4:
time: 32.3 us; the launch traced here: 31.8 us
  Pallas kernels  31.1 us (96%)
  between operations  0.65 us (2%)
    pallas_call x1, Pallas kernels, body(): pl.pallas_call(functools.partial(kernel, (nz, ny, n_tp)), name='mixer', o...  30.4 us
    pallas_call x1, Pallas kernels, body(): pl.pallas_call(leave, name='leave', out_shape=(jax.ShapeDtypeStruct((rb,...  0.72 us

profile of v4, /device:TPU:25, one launch (start us, length us, event | category | flops | bytes accessed | tf_op | source)
XLA Modules:
  0.0 31.8 jit_solution(1500757635135104905)
XLA Ops:
  0.6 30.4 %mixer.1 = (bf16[64,2048]{1,0:T(8,128)(2,1)S(1)}, f32[4,256]{1,0:T(4,128)S(1)}) custom-call(bf16[256,2048]{1,0:T(8,128)(2,1)} %x_hbm.1, bf16[2048,256]{1,0:T(8,128)(2,1)} %wk_hbm.1, bf16[2048,256]{1,0:T(8,128)(2,1)} %wv_hbm.1, bf16[2048,256]{1,0:T(8,128)(2,1)} %wf_hbm.1, bf16[2048,256]{1,0:T(8,128)(2,1)} %wrv_hbm.1, bf16[2048,256]{1,0:T(8,128)(2,1)} %wrq_hbm.1, ...), custom_call_target="tpu_custom_call" | custom-call | tf_op jit(solution)/shard_map/mixer/pallas_call | solution.py:666
  31.0 0.7 %leave.1 = (bf16[64,2048]{1,0:T(8,128)(2,1)}, f32[4,256]{1,0:T(4,128)}) custom-call(bf16[64,2048]{1,0:T(8,128)(2,1)S(1)} %get-tuple-element.6.mixed_v, f32[4,256]{1,0:T(4,128)S(1)} %get-tuple-element.7.log_sum_v), custom_call_target="tpu_custom_call" | custom-call | tf_op jit(solution)/shard_map/leave/pallas_call | solution.py:730

commit v5 on v4

--- a/solution.py
+++ b/solution.py
@@ -54,7 +54,7 @@
     xn, k_src, q_src, v_src, g_src, k_all, v_all, g_all, ga, q_in, s_buf, w_buf, m_s, l_s,
     o_src, lg_src, o_in, lg_in, mix,
     inner, vq, og, ext, st, up_in, up_out, chain_in, chain_out, incoming, part, send2, recv1, recv2,
-    in_gain, q_gain, k_gain, gate_t, a_gain, slack, extra_t, r_gain,
+    in_gain, q_gain, k_gain, gate_t, a_gain, slack, extra_t, r_gain, rec_part,
     load_sem, k_send, v_send, q_send, g_send, k_recv, v_recv, q_recv, g_recv, k_fwd, v_fwd,
     o_send, o_recv, lg_send, lg_recv,
     st_send, st_recv, up_send, up_recv, chain_send, chain_recv,
@@ -539,6 +539,7 @@
         out = out * lax.rsqrt(mean + EPSILON) * r_gain[:, lanes] * og[:, lanes]
         mix[:, cols + j * STATE_ROWS : cols + (j + 1) * STATE_ROWS] = out.astype(BF16)
     loads[9].wait()
+    rec_part[...] = dot(mix[:, cols : 2 * cols], wo_v[cols : 2 * cols, :])
     loads[8].wait()
 
     either(own, lambda ref: landed(ref, o_recv), o_in, heads - 1, heads)
@@ -581,7 +582,9 @@
 
     def partial_of(j, q):
         at = pl.ds(pl.multiple_of(j * 2 * rb, 2 * rb), 2 * rb)
-        part[q, at, :] = dot(mix[at, :], wo_v[:, columns(q)]).astype(BF16)
+        part[q, at, :] = (
+            dot(mix[at, 0:cols], wo_v[0:cols, columns(q)]) + rec_part[at, columns(q)]
+        ).astype(BF16)
         within(j, q).start()
 
     for q in range(splits):
@@ -709,6 +712,7 @@
             pltpu.VMEM((1, cols), F32),
             pltpu.VMEM((rec_heads, rows), F32),
             pltpu.VMEM((1, cols), F32),
+            pltpu.VMEM((rows, width), F32),
             dma((18,)),
             dma, dma, dma, dma,
             *([dma((heads,))] * 3), dma, dma, dma,

time: 32.3 us -> 32.2 us (level)
  no operation moved by 1% of the time
where the time goes in v5:
time: 32.2 us; the launch traced here: 31.6 us
  Pallas kernels  31 us (96%)
  between operations  0.65 us (2%)
    pallas_call x1, Pallas kernels, body(): pl.pallas_call(functools.partial(kernel, (nz, ny, n_tp)), name='mixer', o...  30.3 us
    pallas_call x1, Pallas kernels, body(): pl.pallas_call(leave, name='leave', out_shape=(jax.ShapeDtypeStruct((rb,...  0.72 us

profile of v5, /device:TPU:25, one launch (start us, length us, event | category | flops | bytes accessed | tf_op | source)
XLA Modules:
  0.0 31.6 jit_solution(5622008105602370087)
XLA Ops:
  0.6 30.3 %mixer.1 = (bf16[64,2048]{1,0:T(8,128)(2,1)S(1)}, f32[4,256]{1,0:T(4,128)S(1)}) custom-call(bf16[256,2048]{1,0:T(8,128)(2,1)} %x_hbm.1, bf16[2048,256]{1,0:T(8,128)(2,1)} %wk_hbm.1, bf16[2048,256]{1,0:T(8,128)(2,1)} %wv_hbm.1, bf16[2048,256]{1,0:T(8,128)(2,1)} %wf_hbm.1, bf16[2048,256]{1,0:T(8,128)(2,1)} %wrv_hbm.1, bf16[2048,256]{1,0:T(8,128)(2,1)} %wrq_hbm.1, ...), custom_call_target="tpu_custom_call" | custom-call | tf_op jit(solution)/shard_map/mixer/pallas_call | solution.py:669
  30.9 0.7 %leave.1 = (bf16[64,2048]{1,0:T(8,128)(2,1)}, f32[4,256]{1,0:T(4,128)}) custom-call(bf16[64,2048]{1,0:T(8,128)(2,1)S(1)} %get-tuple-element.6.mixed_v, f32[4,256]{1,0:T(4,128)S(1)} %get-tuple-element.7.log_sum_v), custom_call_target="tpu_custom_call" | custom-call | tf_op jit(solution)/shard_map/leave/pallas_call | solution.py:734
